TPU v7x, 512 devices: a whole 4x8x8 slice. The times are simulated.
512 devices in a mesh: sp: 32 (over z, x), tp: 16 (over y, core).
Axes of the slice: x: 4, y: 8, z: 8, core: 2. Of those that a mesh axis runs over, the one named last changes fastest.
Arguments:
- tokens: bfloat16 [8192, 4096], P('sp', 'tp'), may hold values from -6 to 6
- norm_gain: float32 [2, 4096], replicated, may hold values from 0.1 to 1.9
- w_value: bfloat16 [2, 4096, 2048], P(None, 'sp', 'tp'), may hold values from -0.09375 to 0.09375
- w_gate: bfloat16 [2, 4096, 2048], P(None, 'sp', 'tp'), may hold values from -0.09375 to 0.09375
- conv_taps: float32 [2, 31, 2048], P(None, None, 'tp'), may hold values from -3 to 3
- conv_bias: float32 [2, 2048], P(None, 'tp'), may hold values from -3 to 3
- chan_gain: float32 [2, 2048], P(None, 'tp'), may hold values from 0.1 to 1.9
- chan_bias: float32 [2, 2048], P(None, 'tp'), may hold values from -3 to 3
- w_out: bfloat16 [2, 2048, 4096], P(None, 'sp', 'tp'), may hold values from -0.125 to 0.125
Outputs:
- stream: bfloat16 [8192, 4096], P('sp', 'tp')
All inputs are finite; a program needn't handle non-finite values.
Results may differ from a plain program's by a relative error of at most 0.011.
Values may be sent and summed in bfloat16 or wider, within the bound.
No kernel may reach another device: no remote copies, remote signals or barrier semaphores. Data moves between devices by JAX's collectives and lax.ppermute only.
A program may use at most 64 MiB of HBM per device.

v0:
```python
import functools

import jax
import jax.numpy as jnp
from jax import lax
from jax.experimental import pallas as pl
from jax.experimental.pallas import tpu as pltpu
from jax.sharding import Mesh, PartitionSpec as P


F32 = jnp.float32
BF16 = jnp.bfloat16
HALO = 32
FROM = ((0, 3, -2), (1, 4), (-1, 2, -3))
HBM = pl.BlockSpec(memory_space=pltpu.HBM)
VMEM = pl.BlockSpec(memory_space=pltpu.VMEM)
SMEM = pl.BlockSpec(memory_space=pltpu.SMEM)


def parts_of(x):
    high = x.astype(BF16).astype(F32)
    rest = x - high
    middle = rest.astype(BF16).astype(F32)
    return high, middle, (rest - middle).astype(BF16).astype(F32)


def exchanged(x, axis):
    return lax.all_to_all(x, axis, split_axis=0, concat_axis=0, tiled=True)


def shifted(x, axis, steps):
    count = lax.axis_size(axis)
    return lax.ppermute(x, axis, [(i, (i + steps) % count) for i in range(count)])


def row_dot(ones, x):
    return lax.dot_general(
        ones, x, (((1,), (1,)), ((), ())), precision=lax.Precision.HIGHEST, preferred_element_type=F32
    )


def pack_weights(value, gate, out_weights, first, rest):
    deep, depth = value.shape[1], out_weights.shape[1]
    for copy in range(first.shape[0]):
        first[copy, :, :128] = value[0]
        first[copy, :, 128:] = gate[0]
    rest[:deep, :128] = value[1]
    rest[:deep, 128:] = gate[1]
    rest[deep : deep + depth, :] = out_weights[0]
    rest[deep + depth :, :] = out_weights[1]


def group_kernel(own, third, second, two, three):
    for out in (two, three):
        out[0] = own[...]
        out[1] = third[...]
    three[2] = second[...]


def pack_tokens(earlier, tokens, gains, biases, out, near_gains, near_biases, done):
    rows = tokens.shape[0]
    moves = [
        pltpu.make_async_copy(tokens, out.at[pl.ds(HALO, rows), :], done.at[0]),
        pltpu.make_async_copy(gains, near_gains, done.at[1]),
        pltpu.make_async_copy(biases, near_biases, done.at[2]),
    ]
    for move in moves:
        move.start()
    out[:HALO, :] = earlier[...]
    at = lax.broadcasted_iota(jnp.int32, (16, 256), 0)
    tile = jnp.zeros((16, 256), F32)
    for move in moves:
        move.wait()
    for layer in range(2):
        pair = jnp.concatenate([near_gains[layer : layer + 1, :], near_biases[layer : layer + 1, :]], axis=1)
        for j, part in enumerate(parts_of(pair)):
            tile = jnp.where(at == 3 * layer + j, part, tile)
    out[HALO + rows :, :] = tile.astype(BF16)


def stack_kernel(place, three, ahead, behind, deep, out_first, out_second):
    rows, depth = deep.shape[1], out_first.shape[1]
    for group, steps in zip((three, ahead, behind), FROM, strict=True):
        for j, step in enumerate(steps):
            z = lax.rem(place[2] + 8 - step, 8)
            deep[z] = group[j, :rows, :]
            out_first[z] = group[j, rows : rows + depth, :]
            out_second[z] = group[j, rows + depth :, :]


def join_pieces(place, *refs):
    pieces, out = refs[:-1], refs[-1]
    depth = pieces[0].shape[1]
    for steps, piece in enumerate(pieces):
        source = lax.rem(place[1] + 4 - steps, 4)
        start = pl.multiple_of(lax.rem(source, 2) * depth, depth)
        for y in range(piece.shape[0]):
            out[source // 2, y, pl.ds(start, depth), :] = piece[y]


def join_gathered(weights, out):
    depth = weights.shape[2]
    for c in range(2):
        for h in range(2):
            for y in range(weights.shape[1]):
                out[c, y, h * depth : (h + 1) * depth, :] = weights[2 * c + h, y]


def copy_kernel(x, out):
    for copy in range(out.shape[0]):
        out[copy] = x[:, : out.shape[2], :]


def gated_of(visit, acc, total, squares):
    squares[...] = jnp.zeros(squares.shape, F32)

    def add_squares(block, gain, weights):
        wide = block().astype(F32)
        wide = wide * wide
        squares[...] += wide[:, :128] + wide[:, 128:]

    visit(add_squares)
    scale = lax.rsqrt(jnp.sum(squares[...], axis=1, keepdims=True) / total + 1e-06)
    acc[...] = jnp.zeros(acc.shape, F32)

    def add_product(block, gain, weights):
        normed = (block().astype(F32) * scale * gain()).astype(BF16)
        acc[...] += jnp.dot(normed, weights(), preferred_element_type=F32)

    visit(add_product)
    value = acc[:, :128]
    gate = acc[:, 128:]
    return (value * jax.nn.sigmoid(gate)).astype(BF16)


def convolve_and_pack(extended, taps, bias, layer, out, rows):
    kernel = taps.shape[1]
    convolved = jnp.zeros((rows, 128), F32) + bias[layer : layer + 1, :]
    for k in range(kernel):
        convolved = convolved + taps[layer, k : k + 1, :] * extended[pl.ds(HALO - kernel + 1 + k, rows), :]
    mean = jnp.sum(convolved, axis=1, keepdims=True) * (1.0 / 128.0)
    less = convolved - mean
    ones = jnp.ones((8, 128), F32)
    mean_row = row_dot(ones, convolved) * (1.0 / 128.0)
    square_row = row_dot(ones, less * less)
    at = lax.broadcasted_iota(jnp.int32, (8, 128), 0)
    packed = []
    for row in (mean_row, square_row):
        tile = jnp.zeros((8, 128), F32)
        for j, part in enumerate(parts_of(row)):
            for half in range(2):
                tile = jnp.where(at == 2 * j + half, part[:, half * 128 : half * 128 + 128], tile)
        packed.append(tile)
    small = jnp.concatenate(packed, axis=0).astype(BF16)
    less = less.astype(BF16)
    for copy in range(out.shape[0]):
        out[copy, :rows, :] = less
        out[copy, rows:, :] = small


def first_kernel(rows, tokens, gains, weights, taps, bias, out, acc, squares, extended):
    total = tokens.shape[0] * tokens.shape[2]

    def visit(fn):
        def step(y, carry):
            for c in range(2):
                i = 2 * y + c
                fn(
                    lambda: tokens[i, : HALO + rows, :],
                    lambda: gains[0:1, pl.ds(pl.multiple_of(i * 256, 256), 256)],
                    lambda: jnp.concatenate([weights[2 * c, y], weights[2 * c + 1, y]], axis=0),
                )
            return carry

        lax.fori_loop(0, tokens.shape[0] // 2, step, 0)

    extended[...] = gated_of(visit, acc, total, squares).astype(F32)
    convolve_and_pack(extended, taps, bias, 0, out, rows)


def product_step(block, gain, weights, acc, squares):
    wide = block.astype(F32)
    normed = (wide * gain).astype(BF16)
    wide = wide * wide
    squares[...] += wide[:, :128] + wide[:, 128:]
    acc[...] += jnp.dot(normed, weights, preferred_element_type=F32)


def gate_blocks(groups, place, c, first, gains, weights, acc, squares):
    for blocks, steps in zip(groups, FROM, strict=True):
        for j, step in enumerate(steps):
            y = lax.rem(place[3] + 8 - step, 8)
            gain = gains[1:2, pl.ds(pl.multiple_of((2 * y + c) * 256, 256), 256)]
            depths = jnp.concatenate([weights[2 * c, y], weights[2 * c + 1, y]], axis=0)
            product_step(blocks[j, first:, :], gain, depths, acc, squares)


def gate_own(place, three, ahead, behind, gains, weights, acc, squares):
    acc[...] = jnp.zeros(acc.shape, F32)
    squares[...] = jnp.zeros(squares.shape, F32)
    gate_blocks((three, ahead, behind), place, place[0], 0, gains, weights, acc, squares)


def gate_other(first, place, own_acc, own_squares, three, ahead, behind, gains, weights, out, acc, squares):
    acc[...] = own_acc[first:, :]
    squares[...] = own_squares[first:, :]
    gate_blocks((three, ahead, behind), place, 1 - place[0], first, gains, weights, acc, squares)
    total = 16 * three.shape[2]
    scale = lax.rsqrt(jnp.sum(squares[...], axis=1, keepdims=True) / total + 1e-06)
    value = acc[:, :128] * scale
    gate = acc[:, 128:] * scale
    out[...] = (value * jax.nn.sigmoid(gate)).astype(BF16)


def conv_kernel(rows, earlier, gated, taps, bias, out, extended):
    extended[:HALO, :] = earlier[...].astype(F32)
    extended[HALO:, :] = gated[...].astype(F32)
    convolve_and_pack(extended, taps, bias, 1, out, rows)


def out_kernel(rows, layer, place, own, other, params, stream, joined, out, acc, sides):
    core = place[0]
    count = own.shape[0]
    total = 2 * count * 128

    def stat(tile):
        sums = []
        for half in range(2):
            sums.append(sum(tile[2 * j + half : 2 * j + half + 1, :] for j in range(3)))
        return jnp.concatenate(sums, axis=1)

    means, squares = [], []
    for blocks in (own, other):
        for y in range(count):
            tile = blocks[y, rows:, :].astype(F32)
            means.append(stat(tile[:8]))
            squares.append(stat(tile[8:]))
    means = jnp.concatenate(means, axis=0)
    squares = jnp.concatenate(squares, axis=0)
    center = jnp.mean(means, axis=0, keepdims=True)
    apart = means - center
    spread = jnp.sum(squares + 128.0 * apart * apart, axis=0, keepdims=True) / total
    factor = lax.rsqrt(spread + 1e-05)
    lines = jnp.concatenate([apart * factor, factor, jnp.zeros((128 - 2 * count - 1, rows), F32)], axis=0)
    sides[...] = lines.T

    acc[...] = stream[...].astype(F32)
    wide = jnp.broadcast_to(sides[:, 2 * count : 2 * count + 1], (rows, 128))
    for n, (blocks, c) in enumerate(((own, core), (other, 1 - core))):
        for y in range(count):
            param = params[2 * y + c].astype(F32)
            gain, bias = (
                sum(param[3 * layer + j : 3 * layer + j + 1, k * 128 : k * 128 + 128] for j in range(3))
                for k in range(2)
            )
            side = sides[:, n * count + y : n * count + y + 1]
            shaped = (blocks[y, :rows, :].astype(F32) * wide + side) * gain + bias
            activated = (shaped * jax.nn.sigmoid(shaped)).astype(BF16)
            acc[...] += jnp.dot(activated, joined[c, y], preferred_element_type=F32)
    out[...] = acc[...].astype(BF16)


def call(body, shape, arrays, scratch=(), scalars=0, flops=1_000_000_000, limit=16):
    specs = [VMEM] * arrays if isinstance(arrays, int) else arrays
    return pl.pallas_call(
        body,
        out_shape=shape,
        in_specs=[SMEM] * scalars + specs,
        out_specs=jax.tree.map(lambda _: VMEM, shape),
        scratch_shapes=list(scratch),
        cost_estimate=pl.CostEstimate(flops=flops, bytes_accessed=1_000_000, transcendentals=0),
        compiler_params=pltpu.CompilerParams(vmem_limit_bytes=limit * 1024 * 1024),
    )


def shards(tokens, norm_gain, w_value, w_gate, conv_taps, conv_bias, chan_gain, chan_bias, w_out):
    rows, width = tokens.shape
    ring, deep_ring = lax.axis_size("y"), lax.axis_size("z")
    place = jnp.stack([lax.axis_index(axis).astype(jnp.int32) for axis in ("c", "x", "z", "y")])
    blocks = deep_ring * lax.axis_size("x")
    onward = [(i, i + 1) for i in range(blocks - 1)]
    deep, depth = w_value.shape[1], w_out.shape[1]

    earlier = lax.ppermute(tokens[rows - HALO :], ("z", "x"), onward)
    packed = call(
        pack_tokens,
        jax.ShapeDtypeStruct((HALO + rows + 16, width), BF16),
        [VMEM, HBM, HBM, HBM],
        scratch=[
            pltpu.VMEM(chan_gain.shape, F32),
            pltpu.VMEM(chan_bias.shape, F32),
            pltpu.SemaphoreType.DMA((3,)),
        ],
        limit=60,
    )(earlier, tokens, chan_gain, chan_bias)
    everything = lax.all_gather(packed, ("y", "c"))
    params = everything[:, HALO + rows :]

    def relay(x, axis):
        third, second = shifted(x, axis, 3), shifted(x, axis, -2)
        two, three = call(
            group_kernel, (jax.ShapeDtypeStruct((2, *x.shape), BF16), jax.ShapeDtypeStruct((3, *x.shape), BF16)), 3
        )(x, third, second)
        return three, shifted(two, axis, 1), shifted(three, axis, -1)

    first, rest = call(
        pack_weights,
        (jax.ShapeDtypeStruct((deep_ring, deep, width), BF16), jax.ShapeDtypeStruct((deep + 2 * depth, width), BF16)),
        3,
    )(w_value, w_gate, w_out)
    first = exchanged(first, "z")
    in_first = call(copy_kernel, jax.ShapeDtypeStruct((lax.axis_size("x"), deep_ring, deep, width), BF16), 1)(first)
    in_first = exchanged(in_first, "x")
    groups = relay(rest, "z")
    out_shape = jax.ShapeDtypeStruct((deep_ring, depth, width), BF16)
    in_second, out_first, out_second = call(
        stack_kernel, (jax.ShapeDtypeStruct((deep_ring, deep, width), BF16), out_shape, out_shape), 3, scalars=1
    )(place, *groups)
    joined_shape = jax.ShapeDtypeStruct((2, deep_ring, 2 * depth, width), BF16)
    pieces = [shifted(out_first, "x", steps) for steps in (1, 2, 3)]
    joined_first = call(join_pieces, joined_shape, 4, scalars=1)(place, out_first, *pieces)
    in_second = lax.all_gather(in_second, "x")
    out_second = lax.all_gather(out_second, "x")
    joined_second = call(join_gathered, joined_shape, 1)(out_second)

    packed_shape = jax.ShapeDtypeStruct((ring, rows + 16, 128), BF16)
    packed = call(
        functools.partial(first_kernel, rows),
        packed_shape,
        5,
        scratch=[
            pltpu.VMEM((HALO + rows, 256), F32),
            pltpu.VMEM((HALO + rows, 128), F32),
            pltpu.VMEM((HALO + rows, 128), F32),
        ],
        flops=4_000_000_000,
    )(everything, norm_gain, in_first, conv_taps, conv_bias)

    def out_step(own, other, stream, layer, joined):
        return call(
            functools.partial(out_kernel, rows, layer),
            jax.ShapeDtypeStruct((rows, width), BF16),
            5,
            scratch=[pltpu.VMEM((rows, width), F32), pltpu.VMEM((rows, 128), F32)],
            scalars=1,
            flops=4_000_000_000,
        )(place, own, other, params, stream, joined)

    own = exchanged(packed, "y")
    other = shifted(own, "c", 1)
    stream = out_step(own, other, tokens, 0, joined_first)
    own = relay(stream, "y")
    other = [shifted(group, "c", 1) for group in own]
    sums = (jax.ShapeDtypeStruct((rows, 256), F32), jax.ShapeDtypeStruct((rows, 128), F32))
    acc, squares = call(gate_own, sums, 5, scalars=1, flops=4_000_000_000)(place, *own, norm_gain, in_second)

    def gate_rest(first):
        return call(
            functools.partial(gate_other, first),
            jax.ShapeDtypeStruct((rows - first, 128), BF16),
            7,
            scratch=[pltpu.VMEM((rows - first, 256), F32), pltpu.VMEM((rows - first, 128), F32)],
            scalars=1,
            flops=4_000_000_000,
        )(place, acc, squares, *other, norm_gain, in_second)

    last = gate_rest(rows - HALO)
    earlier = lax.ppermute(last, ("z", "x"), onward)
    gated = gate_rest(0)
    packed = call(
        functools.partial(conv_kernel, rows), packed_shape, 4, scratch=[pltpu.VMEM((HALO + rows, 128), F32)]
    )(earlier, gated, conv_taps, conv_bias)
    own = exchanged(packed, "y")
    other = shifted(own, "c", 1)
    return out_step(own, other, stream, 1, joined_second)


def solution(mesh):
    grid = Mesh(mesh.devices.reshape(8, 4, 8, 2), ("z", "x", "y", "c"))
    sp, tp = ("z", "x"), ("y", "c")
    placed = (
        P(sp, tp),
        P(),
        P(None, sp, tp),
        P(None, sp, tp),
        P(None, None, tp),
        P(None, tp),
        P(None, tp),
        P(None, tp),
        P(None, sp, tp),
    )
    return jax.shard_map(shards, mesh=grid, in_specs=placed, out_specs=P(sp, tp), check_vma=False)
```

profile of v0, /device:TPU:65, one launch (start us, length us, event | category | flops | bytes accessed | tf_op | source)
XLA Modules:
  0.0 208.3 jit_solution(17565589858689582090)
XLA Ops:
  6.5 0.8 slice.6
  7.3 3.1 %collective-permute-start = (bf16[32,256]{1,0:T(8,128)(2,1)S(1)}, bf16[32,256]{1,0:T(8,128)(2,1)S(1)}, u32[]{:S(2)}, u32[]{:S(2)}) collective-permute-start(bf16[32,256]{1,0:T(8,128)(2,1)S(1)} %slice.6), channel_id=1, source_target_pairs={{0,16},{16,32},{32,48},{48,64},{64,80},{80,96},{96,112},{112,128},... | collective-permute-start | bytes 49160 | tf_op jit(solution)/shard_map/ppermute | solution.py:284
  10.4 3.5 %collective-permute-done.earlier = bf16[32,256]{1,0:T(8,128)(2,1)S(1)} collective-permute-done((bf16[32,256]{1,0:T(8,128)(2,1)S(1)}, bf16[32,256]{1,0:T(8,128)(2,1)S(1)}, u32[]{:S(2)}, u32[]{:S(2)}) %collective-permute-start) | collective-permute-done | bytes 16416 | tf_op jit(solution)/shard_map/ppermute | solution.py:284
  13.9 0.6 copy-done.11
  14.5 2.3 %shard_map.91 = bf16[304,256]{1,0:T(8,128)(2,1)} custom-call(bf16[32,256]{1,0:T(8,128)(2,1)} %copy-done.11, bf16[256,256]{1,0:T(8,128)(2,1)} %stream.1, f32[2,128]{1,0:T(2,128)} %gains.5, f32[2,128]{1,0:T(2,128)} %biases.1), custom_call_target="tpu_custom_call" | custom-call | flops 1000000000 | bytes 1000000 | tf_op jit(solution)/shard_map/pallas_call | solution.py:285
  16.8 0.0 all-gather.7.cloned.1.call-update
  16.9 0.1 shard_map.92
  17.0 23.9 %all_to_all.20.x = bf16[8,128,256]{2,1,0:T(8,128)(2,1)S(1)} all-to-all(bf16[8,128,256]{2,1,0:T(8,128)(2,1)S(1)} %get-tuple-element.16), channel_id=1, replica_groups=mesh['z'=8,'x'=4,'y'=8,'c'=2] {'z'}, dimensions={0} | all-to-all | bytes 1048576 | tf_op jit(solution)/shard_map/all_to_all | solution.py:28
  40.9 0.1 shard_map.93
  41.1 1.3 copy-done
  42.4 3.6 %all-to-all-start.1 = ((bf16[4,8,128,256]{3,2,1,0:T(8,128)(2,1)}), bf16[4,8,128,256]{3,2,1,0:T(8,128)(2,1)S(1)}, u32[]{:S(2)}, u32[]{:S(2)}) async-start(bf16[4,8,128,256]{3,2,1,0:T(8,128)(2,1)} %copy-done), calls=%async_computation.1 | async-start | bytes 4194304 | tf_op jit(solution)/shard_map/all_to_all | solution.py:28
  46.0 0.0 all-gather.9.cloned.1.call-start
  46.1 2.7 %collective-permute-start.2 = (bf16[256,256]{1,0:T(8,128)(2,1)S(1)}, bf16[256,256]{1,0:T(8,128)(2,1)S(1)}, u32[]{:S(2)}, u32[]{:S(2)}) collective-permute-start(bf16[256,256]{1,0:T(8,128)(2,1)S(1)} %get-tuple-element.17.own), channel_id=1, source_target_pairs={{0,192},{64,256},{128,320},{192,384},{256,448},{320,0},{384,64},{4... | collective-permute-start | bytes 393224 | tf_op jit(solution)/shard_map/ppermute | solution.py:33
  48.8 4.5 %collective-permute-start.3 = (bf16[256,256]{1,0:T(8,128)(2,1)S(1)}, bf16[256,256]{1,0:T(8,128)(2,1)S(1)}, u32[]{:S(2)}, u32[]{:S(2)}) collective-permute-start(bf16[256,256]{1,0:T(8,128)(2,1)S(1)} %get-tuple-element.17.own), channel_id=1, source_target_pairs={{0,384},{64,448},{128,0},{192,64},{256,128},{320,192},{384,256},{4... | collective-permute-start | bytes 393224 | tf_op jit(solution)/shard_map/ppermute | solution.py:33
  53.3 4.0 %collective-permute-done.2.third = bf16[256,256]{1,0:T(8,128)(2,1)S(1)} collective-permute-done((bf16[256,256]{1,0:T(8,128)(2,1)S(1)}, bf16[256,256]{1,0:T(8,128)(2,1)S(1)}, u32[]{:S(2)}, u32[]{:S(2)}) %collective-permute-start.2) | collective-permute-done | bytes 131104 | tf_op jit(solution)/shard_map/ppermute | solution.py:33
  57.3 0.9 collective-permute-done.3.second
  58.2 2.9 %collective-permute-start.5 = (bf16[3,256,256]{2,1,0:T(8,128)(2,1)S(1)}, bf16[3,256,256]{2,1,0:T(8,128)(2,1)S(1)}, u32[]{:S(2)}, u32[]{:S(2)}) collective-permute-start(bf16[3,256,256]{2,1,0:T(8,128)(2,1)S(1)} %get-tuple-element.18.three), channel_id=1, source_target_pairs={{0,448},{64,0},{128,64},{192,128},{256,192},{320,256},{384,320},{4... | collective-permute-start | bytes 1179656 | tf_op jit(solution)/shard_map/ppermute | solution.py:33
  61.1 2.4 %collective-permute-start.4 = (bf16[2,256,256]{2,1,0:T(8,128)(2,1)S(1)}, bf16[2,256,256]{2,1,0:T(8,128)(2,1)S(1)}, u32[]{:S(2)}, u32[]{:S(2)}) collective-permute-start(bf16[2,256,256]{2,1,0:T(8,128)(2,1)S(1)} %get-tuple-element.19), channel_id=1, source_target_pairs={{0,64},{64,128},{128,192},{192,256},{256,320},{320,384},{384,448},... | collective-permute-start | bytes 786440 | tf_op jit(solution)/shard_map/ppermute | solution.py:33
  63.5 0.1 pad_add_fusion.place
  63.6 5.2 %collective-permute-done.4.ahead = bf16[2,256,256]{2,1,0:T(8,128)(2,1)S(1)} collective-permute-done((bf16[2,256,256]{2,1,0:T(8,128)(2,1)S(1)}, bf16[2,256,256]{2,1,0:T(8,128)(2,1)S(1)}, u32[]{:S(2)}, u32[]{:S(2)}) %collective-permute-start.4) | collective-permute-done | bytes 262176 | tf_op jit(solution)/shard_map/ppermute | solution.py:33
  68.8 0.0 collective-permute-done.5.behind
  68.8 1.5 shard_map.96
  70.3 0.0 all-gather.9.cloned.1.call-update
  70.4 0.0 all-gather.11.cloned.1.call-start
  70.4 0.0 all-gather.7.cloned.1.call-done
  70.5 1.7 copy-done.1
  72.2 3.4 %shard_map.94 = bf16[8,272,128]{2,1,0:T(8,128)(2,1)S(1)} custom-call(bf16[16,304,256]{2,1,0:T(8,128)(2,1)S(1)} %bitcast.8, f32[2,4096]{1,0:T(2,128)S(1)} %copy-done.8, bf16[4,8,128,256]{3,2,1,0:T(8,128)(2,1)S(1)} %all-to-all-done.1.weights, f32[2,31,128]{2,1,0:T(8,128)S(1)} %copy.12.taps, f32[2,128]{1,0:T(2,128)S(1)} %copy-done.9), custom_call_target="tpu_custom_call" | custom-call | flops 4000000000 | bytes 1000000 | tf_op jit(solution)/shard_map/pallas_call | solution.py:327
  75.6 19.2 %all_to_all.21.own = bf16[8,272,128]{2,1,0:T(8,128)(2,1)S(1)} all-to-all(bf16[8,272,128]{2,1,0:T(8,128)(2,1)S(1)} %shard_map.94), channel_id=1, replica_groups=mesh['z'=8,'x'=4,'y'=8,'c'=2] {'y'}, dimensions={0} | all-to-all | bytes 1114112 | tf_op jit(solution)/shard_map/all_to_all | solution.py:28
  94.8 9.2 %collective-permute-start.1 = (bf16[8,272,128]{2,1,0:T(8,128)(2,1)S(1)}, bf16[8,272,128]{2,1,0:T(8,128)(2,1)S(1)}, u32[]{:S(2)}, u32[]{:S(2)}) collective-permute-start(bf16[8,272,128]{2,1,0:T(8,128)(2,1)S(1)} %all_to_all.21.own), channel_id=1, source_target_pairs={{0,1},{1,0},{2,3},{3,2},{4,5},{5,4},{6,7},{7,6},{8,9},{9,8},{10,11... | collective-permute-start | bytes 1671176 | tf_op jit(solution)/shard_map/ppermute | solution.py:33
  104.0 3.4 %collective-permute-start.6 = (bf16[8,64,256]{2,1,0:T(8,128)(2,1)S(1)}, bf16[8,64,256]{2,1,0:T(8,128)(2,1)S(1)}, u32[]{:S(2)}, u32[]{:S(2)}) collective-permute-start(bf16[8,64,256]{2,1,0:T(8,128)(2,1)S(1)} %get-tuple-element.20.refs_0_), channel_id=1, source_target_pairs={{0,16},{16,32},{32,48},{48,0},{1,17},{17,33},{33,49},{49,1},{2,18}... | collective-permute-start | bytes 786440 | tf_op jit(solution)/shard_map/ppermute | solution.py:33
  107.4 4.2 %collective-permute-start.7 = (bf16[8,64,256]{2,1,0:T(8,128)(2,1)S(1)}, bf16[8,64,256]{2,1,0:T(8,128)(2,1)S(1)}, u32[]{:S(2)}, u32[]{:S(2)}) collective-permute-start(bf16[8,64,256]{2,1,0:T(8,128)(2,1)S(1)} %get-tuple-element.20.refs_0_), channel_id=1, source_target_pairs={{0,32},{16,48},{32,0},{48,16},{1,33},{17,49},{33,1},{49,17},{2,34}... | collective-permute-start | bytes 786440 | tf_op jit(solution)/shard_map/ppermute | solution.py:33
  111.6 3.2 %collective-permute-start.8 = (bf16[8,64,256]{2,1,0:T(8,128)(2,1)S(1)}, bf16[8,64,256]{2,1,0:T(8,128)(2,1)S(1)}, u32[]{:S(2)}, u32[]{:S(2)}) collective-permute-start(bf16[8,64,256]{2,1,0:T(8,128)(2,1)S(1)} %get-tuple-element.20.refs_0_), channel_id=1, source_target_pairs={{0,48},{16,0},{32,16},{48,32},{1,49},{17,1},{33,17},{49,33},{2,50}... | collective-permute-start | bytes 786440 | tf_op jit(solution)/shard_map/ppermute | solution.py:33
  114.8 3.7 %collective-permute-done.6.refs_1_ = bf16[8,64,256]{2,1,0:T(8,128)(2,1)S(1)} collective-permute-done((bf16[8,64,256]{2,1,0:T(8,128)(2,1)S(1)}, bf16[8,64,256]{2,1,0:T(8,128)(2,1)S(1)}, u32[]{:S(2)}, u32[]{:S(2)}) %collective-permute-start.6) | collective-permute-done | bytes 262176 | tf_op jit(solution)/shard_map/ppermute | solution.py:33
  118.5 5.9 %collective-permute-done.7.refs_2_ = bf16[8,64,256]{2,1,0:T(8,128)(2,1)S(1)} collective-permute-done((bf16[8,64,256]{2,1,0:T(8,128)(2,1)S(1)}, bf16[8,64,256]{2,1,0:T(8,128)(2,1)S(1)}, u32[]{:S(2)}, u32[]{:S(2)}) %collective-permute-start.7) | collective-permute-done | bytes 262176 | tf_op jit(solution)/shard_map/ppermute | solution.py:33
  124.4 0.6 shard_map.97.joined
  125.0 0.9 slice.8.params
  126.0 1.7 shard_map.98.own.stream
  127.7 5.0 %collective-permute-start.9 = (bf16[256,256]{1,0:T(8,128)(2,1)S(1)}, bf16[256,256]{1,0:T(8,128)(2,1)S(1)}, u32[]{:S(2)}, u32[]{:S(2)}) collective-permute-start(bf16[256,256]{1,0:T(8,128)(2,1)S(1)} %shard_map.98.own.stream), channel_id=1, source_target_pairs={{0,6},{2,8},{4,10},{6,12},{8,14},{10,0},{12,2},{14,4},{1,7},{3,9},... | collective-permute-start | bytes 393224 | tf_op jit(solution)/shard_map/ppermute | solution.py:33
  132.6 3.4 %collective-permute-start.10 = (bf16[256,256]{1,0:T(8,128)(2,1)S(1)}, bf16[256,256]{1,0:T(8,128)(2,1)S(1)}, u32[]{:S(2)}, u32[]{:S(2)}) collective-permute-start(bf16[256,256]{1,0:T(8,128)(2,1)S(1)} %shard_map.98.own.stream), channel_id=1, source_target_pairs={{0,12},{2,14},{4,0},{6,2},{8,4},{10,6},{12,8},{14,10},{1,13},{3,15... | collective-permute-start | bytes 393224 | tf_op jit(solution)/shard_map/ppermute | solution.py:33
  136.0 6.1 %collective-permute-done.9.third = bf16[256,256]{1,0:T(8,128)(2,1)S(1)} collective-permute-done((bf16[256,256]{1,0:T(8,128)(2,1)S(1)}, bf16[256,256]{1,0:T(8,128)(2,1)S(1)}, u32[]{:S(2)}, u32[]{:S(2)}) %collective-permute-start.9) | collective-permute-done | bytes 131104 | tf_op jit(solution)/shard_map/ppermute | solution.py:33
  142.1 0.0 collective-permute-done.10.second
  142.2 5.9 %collective-permute-start.12 = (bf16[3,256,256]{2,1,0:T(8,128)(2,1)S(1)}, bf16[3,256,256]{2,1,0:T(8,128)(2,1)S(1)}, u32[]{:S(2)}, u32[]{:S(2)}) collective-permute-start(bf16[3,256,256]{2,1,0:T(8,128)(2,1)S(1)} %get-tuple-element.21.three), channel_id=1, source_target_pairs={{0,14},{2,0},{4,2},{6,4},{8,6},{10,8},{12,10},{14,12},{1,15},{3,1}... | collective-permute-start | bytes 1179656 | tf_op jit(solution)/shard_map/ppermute | solution.py:33
  148.1 1.9 collective-permute-start.11
  150.0 2.7 %collective-permute-start.13 = (bf16[3,256,256]{2,1,0:T(8,128)(2,1)S(1)}, bf16[3,256,256]{2,1,0:T(8,128)(2,1)S(1)}, u32[]{:S(2)}, u32[]{:S(2)}) collective-permute-start(bf16[3,256,256]{2,1,0:T(8,128)(2,1)S(1)} %get-tuple-element.21.three), channel_id=1, source_target_pairs={{0,1},{1,0},{2,3},{3,2},{4,5},{5,4},{6,7},{7,6},{8,9},{9,8},{10,11... | collective-permute-start | bytes 1179656 | tf_op jit(solution)/shard_map/ppermute | solution.py:33
  152.7 3.3 %collective-permute-done.12.behind = bf16[3,256,256]{2,1,0:T(8,128)(2,1)S(1)} collective-permute-done((bf16[3,256,256]{2,1,0:T(8,128)(2,1)S(1)}, bf16[3,256,256]{2,1,0:T(8,128)(2,1)S(1)}, u32[]{:S(2)}, u32[]{:S(2)}) %collective-permute-start.12) | collective-permute-done | bytes 393248 | tf_op jit(solution)/shard_map/ppermute | solution.py:33
  156.1 3.2 %collective-permute-start.15 = (bf16[3,256,256]{2,1,0:T(8,128)(2,1)S(1)}, bf16[3,256,256]{2,1,0:T(8,128)(2,1)S(1)}, u32[]{:S(2)}, u32[]{:S(2)}) collective-permute-start(bf16[3,256,256]{2,1,0:T(8,128)(2,1)S(1)} %collective-permute-done.12.behind), channel_id=1, source_target_pairs={{0,1},{1,0},{2,3},{3,2},{4,5},{5,4},{6,7},{7,6},{8,9},{9,8},{10,11... | collective-permute-start | bytes 1179656 | tf_op jit(solution)/shard_map/ppermute | solution.py:33
  159.3 0.0 all-gather.11.cloned.1.call-update
  159.3 0.0 collective-permute-done.11.ahead
  159.4 2.5 %collective-permute-start.14 = (bf16[2,256,256]{2,1,0:T(8,128)(2,1)S(1)}, bf16[2,256,256]{2,1,0:T(8,128)(2,1)S(1)}, u32[]{:S(2)}, u32[]{:S(2)}) collective-permute-start(bf16[2,256,256]{2,1,0:T(8,128)(2,1)S(1)} %collective-permute-done.11.ahead), channel_id=1, source_target_pairs={{0,1},{1,0},{2,3},{3,2},{4,5},{5,4},{6,7},{7,6},{8,9},{9,8},{10,11... | collective-permute-start | bytes 786440 | tf_op jit(solution)/shard_map/ppermute | solution.py:33
  161.8 0.0 all-gather.9.cloned.1.call-done
  161.9 1.6 copy-done.3
  163.5 1.0 shard_map.100
  164.5 0.8 shard_map.101
  165.4 1.9 collective-permute-start.16
  167.3 1.0 shard_map.102.gated
  168.4 3.5 %collective-permute-done.16.earlier = bf16[32,128]{1,0:T(8,128)(2,1)S(1)} collective-permute-done((bf16[32,128]{1,0:T(8,128)(2,1)S(1)}, bf16[32,128]{1,0:T(8,128)(2,1)S(1)}, u32[]{:S(2)}, u32[]{:S(2)}) %collective-permute-start.16) | collective-permute-done | bytes 8224 | tf_op jit(solution)/shard_map/ppermute | solution.py:368
  171.9 0.7 shard_map.103
  172.6 19.2 %all_to_all.22.own = bf16[8,272,128]{2,1,0:T(8,128)(2,1)S(1)} all-to-all(bf16[8,272,128]{2,1,0:T(8,128)(2,1)S(1)} %shard_map.103), channel_id=1, replica_groups=mesh['z'=8,'x'=4,'y'=8,'c'=2] {'y'}, dimensions={0} | all-to-all | bytes 1114112 | tf_op jit(solution)/shard_map/all_to_all | solution.py:28
  191.9 6.0 %collective-permute-start.17 = (bf16[8,272,128]{2,1,0:T(8,128)(2,1)S(1)}, bf16[8,272,128]{2,1,0:T(8,128)(2,1)S(1)}, u32[]{:S(2)}, u32[]{:S(2)}) collective-permute-start(bf16[8,272,128]{2,1,0:T(8,128)(2,1)S(1)} %all_to_all.22.own), channel_id=1, source_target_pairs={{0,1},{1,0},{2,3},{3,2},{4,5},{5,4},{6,7},{7,6},{8,9},{9,8},{10,11... | collective-permute-start | bytes 1671176 | tf_op jit(solution)/shard_map/ppermute | solution.py:33
  197.8 0.0 all-gather.11.cloned.1.call-done
  197.9 1.2 copy-done.4
  199.1 0.1 shard_map.104.joined
  199.2 0.2 collective-permute-done.17.other
  199.4 2.3 %shard_map.105 = bf16[256,256]{1,0:T(8,128)(2,1)} custom-call(s32[4]{0:T(128)S(1)} %pad_add_fusion.place, bf16[8,272,128]{2,1,0:T(8,128)(2,1)S(1)} %all_to_all.22.own, bf16[8,272,128]{2,1,0:T(8,128)(2,1)S(1)} %collective-permute-done.17.other, bf16[16,16,256]{2,1,0:T(8,128)(2,1)S(1)} %slice.8.params, bf16[256,256]{1,0:T(8,128)(2,1)S(1)} %shard_map.98.own.stream, ...), custom_call_target="tpu_custom_call" | custom-call | flops 4000000000 | bytes 1000000 | tf_op jit(solution)/shard_map/pallas_call | solution.py:340
  (29 shorter events, 0.1 us)
Async XLA Ops:
  6.5 10.3 %copy-start.5 = (bf16[2,128,128]{2,1,0:T(8,128)(2,1)S(1)}, bf16[2,128,128]{2,1,0:T(8,128)(2,1)}, u32[]{:S(2)}) copy-start(bf16[2,128,128]{2,1,0:T(8,128)(2,1)} %value.1) | copy-start | bytes 196612
  6.5 10.3 %copy-start.6 = (bf16[2,128,128]{2,1,0:T(8,128)(2,1)S(1)}, bf16[2,128,128]{2,1,0:T(8,128)(2,1)}, u32[]{:S(2)}) copy-start(bf16[2,128,128]{2,1,0:T(8,128)(2,1)} %gate.1) | copy-start | bytes 196612
  6.5 10.3 %copy-start.7 = (bf16[2,64,256]{2,1,0:T(8,128)(2,1)S(1)}, bf16[2,64,256]{2,1,0:T(8,128)(2,1)}, u32[]{:S(2)}) copy-start(bf16[2,64,256]{2,1,0:T(8,128)(2,1)} %out_weights.1) | copy-start | bytes 196612
  6.5 63.9 %all-gather.7.cloned.1.call-start = ((), (), s32[]{:S(2)}) async-start(), calls=%async_computation.4 | async-start | bytes 2646016 | tf_op jit(solution)/shard_map/all_gather | solution.py:296
  7.3 6.6 %collective-permute-start = (bf16[32,256]{1,0:T(8,128)(2,1)S(1)}, bf16[32,256]{1,0:T(8,128)(2,1)S(1)}, u32[]{:S(2)}, u32[]{:S(2)}) collective-permute-start(bf16[32,256]{1,0:T(8,128)(2,1)S(1)} %slice.6), channel_id=1, source_target_pairs={{0,16},{16,32},{32,48},{48,64},{64,80},{80,96},{96,112},{112,128},... | collective-permute-start | bytes 49160 | tf_op jit(solution)/shard_map/ppermute | solution.py:284
  13.9 0.6 copy-start.11
  41.1 1.3 copy-start
  42.4 28.0 %all-to-all-start.1 = ((bf16[4,8,128,256]{3,2,1,0:T(8,128)(2,1)}), bf16[4,8,128,256]{3,2,1,0:T(8,128)(2,1)S(1)}, u32[]{:S(2)}, u32[]{:S(2)}) async-start(bf16[4,8,128,256]{3,2,1,0:T(8,128)(2,1)} %copy-done), calls=%async_computation.1 | async-start | bytes 4194304 | tf_op jit(solution)/shard_map/all_to_all | solution.py:28
  46.0 115.8 %all-gather.9.cloned.1.call-start = ((), (), s32[]{:S(2)}) async-start(), calls=%async_computation.5 | async-start | bytes 2621440 | tf_op jit(solution)/shard_map/all_gather | solution.py:322
  46.1 11.2 %collective-permute-start.2 = (bf16[256,256]{1,0:T(8,128)(2,1)S(1)}, bf16[256,256]{1,0:T(8,128)(2,1)S(1)}, u32[]{:S(2)}, u32[]{:S(2)}) collective-permute-start(bf16[256,256]{1,0:T(8,128)(2,1)S(1)} %get-tuple-element.17.own), channel_id=1, source_target_pairs={{0,192},{64,256},{128,320},{192,384},{256,448},{320,0},{384,64},{4... | collective-permute-start | bytes 393224 | tf_op jit(solution)/shard_map/ppermute | solution.py:33
  48.8 9.4 %collective-permute-start.3 = (bf16[256,256]{1,0:T(8,128)(2,1)S(1)}, bf16[256,256]{1,0:T(8,128)(2,1)S(1)}, u32[]{:S(2)}, u32[]{:S(2)}) collective-permute-start(bf16[256,256]{1,0:T(8,128)(2,1)S(1)} %get-tuple-element.17.own), channel_id=1, source_target_pairs={{0,384},{64,448},{128,0},{192,64},{256,128},{320,192},{384,256},{4... | collective-permute-start | bytes 393224 | tf_op jit(solution)/shard_map/ppermute | solution.py:33
  58.2 10.6 %collective-permute-start.5 = (bf16[3,256,256]{2,1,0:T(8,128)(2,1)S(1)}, bf16[3,256,256]{2,1,0:T(8,128)(2,1)S(1)}, u32[]{:S(2)}, u32[]{:S(2)}) collective-permute-start(bf16[3,256,256]{2,1,0:T(8,128)(2,1)S(1)} %get-tuple-element.18.three), channel_id=1, source_target_pairs={{0,448},{64,0},{128,64},{192,128},{256,192},{320,256},{384,320},{4... | collective-permute-start | bytes 1179656 | tf_op jit(solution)/shard_map/ppermute | solution.py:33
  61.1 7.7 %collective-permute-start.4 = (bf16[2,256,256]{2,1,0:T(8,128)(2,1)S(1)}, bf16[2,256,256]{2,1,0:T(8,128)(2,1)S(1)}, u32[]{:S(2)}, u32[]{:S(2)}) collective-permute-start(bf16[2,256,256]{2,1,0:T(8,128)(2,1)S(1)} %get-tuple-element.19), channel_id=1, source_target_pairs={{0,64},{64,128},{128,192},{192,256},{256,320},{320,384},{384,448},... | collective-permute-start | bytes 786440 | tf_op jit(solution)/shard_map/ppermute | solution.py:33
  63.6 6.8 %copy-start.10 = (f32[2,31,128]{2,0,1:T(2,128)S(1)}, f32[2,31,128]{2,0,1:T(2,128)}, u32[]{:S(2)}) copy-start(f32[2,31,128]{2,0,1:T(2,128)} %param.13) | copy-start | bytes 95236
  63.6 6.8 %copy-start.8 = (f32[2,4096]{1,0:T(2,128)S(1)}, f32[2,4096]{1,0:T(2,128)}, u32[]{:S(2)}) copy-start(f32[2,4096]{1,0:T(2,128)} %gains.9) | copy-start | bytes 98308
  63.6 6.9 %copy-start.9 = (f32[2,128]{1,0:T(2,128)S(1)}, f32[2,128]{1,0:T(2,128)}, u32[]{:S(2)}) copy-start(f32[2,128]{1,0:T(2,128)} %bias.3) | copy-start | bytes 3076
  70.4 127.5 %all-gather.11.cloned.1.call-start = ((), (), s32[]{:S(2)}) async-start(), calls=%async_computation.6 | async-start | bytes 1310720 | tf_op jit(solution)/shard_map/all_gather | solution.py:323
  70.5 1.7 copy-start.1
  94.8 31.2 %copy-start.2 = (bf16[256,256]{1,0:T(8,128)(2,1)S(1)}, bf16[256,256]{1,0:T(8,128)(2,1)}, u32[]{:S(2)}) copy-start(bf16[256,256]{1,0:T(8,128)(2,1)} %stream.1) | copy-start | bytes 393220
  94.8 31.2 %collective-permute-start.1 = (bf16[8,272,128]{2,1,0:T(8,128)(2,1)S(1)}, bf16[8,272,128]{2,1,0:T(8,128)(2,1)S(1)}, u32[]{:S(2)}, u32[]{:S(2)}) collective-permute-start(bf16[8,272,128]{2,1,0:T(8,128)(2,1)S(1)} %all_to_all.21.own), channel_id=1, source_target_pairs={{0,1},{1,0},{2,3},{3,2},{4,5},{5,4},{6,7},{7,6},{8,9},{9,8},{10,11... | collective-permute-start | bytes 1671176 | tf_op jit(solution)/shard_map/ppermute | solution.py:33
  104.0 14.5 %collective-permute-start.6 = (bf16[8,64,256]{2,1,0:T(8,128)(2,1)S(1)}, bf16[8,64,256]{2,1,0:T(8,128)(2,1)S(1)}, u32[]{:S(2)}, u32[]{:S(2)}) collective-permute-start(bf16[8,64,256]{2,1,0:T(8,128)(2,1)S(1)} %get-tuple-element.20.refs_0_), channel_id=1, source_target_pairs={{0,16},{16,32},{32,48},{48,0},{1,17},{17,33},{33,49},{49,1},{2,18}... | collective-permute-start | bytes 786440 | tf_op jit(solution)/shard_map/ppermute | solution.py:33
  107.4 17.0 %collective-permute-start.7 = (bf16[8,64,256]{2,1,0:T(8,128)(2,1)S(1)}, bf16[8,64,256]{2,1,0:T(8,128)(2,1)S(1)}, u32[]{:S(2)}, u32[]{:S(2)}) collective-permute-start(bf16[8,64,256]{2,1,0:T(8,128)(2,1)S(1)} %get-tuple-element.20.refs_0_), channel_id=1, source_target_pairs={{0,32},{16,48},{32,0},{48,16},{1,33},{17,49},{33,1},{49,17},{2,34}... | collective-permute-start | bytes 786440 | tf_op jit(solution)/shard_map/ppermute | solution.py:33
  111.6 12.8 %collective-permute-start.8 = (bf16[8,64,256]{2,1,0:T(8,128)(2,1)S(1)}, bf16[8,64,256]{2,1,0:T(8,128)(2,1)S(1)}, u32[]{:S(2)}, u32[]{:S(2)}) collective-permute-start(bf16[8,64,256]{2,1,0:T(8,128)(2,1)S(1)} %get-tuple-element.20.refs_0_), channel_id=1, source_target_pairs={{0,48},{16,0},{32,16},{48,32},{1,49},{17,1},{33,17},{49,33},{2,50}... | collective-permute-start | bytes 786440 | tf_op jit(solution)/shard_map/ppermute | solution.py:33
  127.7 14.4 %collective-permute-start.9 = (bf16[256,256]{1,0:T(8,128)(2,1)S(1)}, bf16[256,256]{1,0:T(8,128)(2,1)S(1)}, u32[]{:S(2)}, u32[]{:S(2)}) collective-permute-start(bf16[256,256]{1,0:T(8,128)(2,1)S(1)} %shard_map.98.own.stream), channel_id=1, source_target_pairs={{0,6},{2,8},{4,10},{6,12},{8,14},{10,0},{12,2},{14,4},{1,7},{3,9},... | collective-permute-start | bytes 393224 | tf_op jit(solution)/shard_map/ppermute | solution.py:33
  132.6 9.5 %collective-permute-start.10 = (bf16[256,256]{1,0:T(8,128)(2,1)S(1)}, bf16[256,256]{1,0:T(8,128)(2,1)S(1)}, u32[]{:S(2)}, u32[]{:S(2)}) collective-permute-start(bf16[256,256]{1,0:T(8,128)(2,1)S(1)} %shard_map.98.own.stream), channel_id=1, source_target_pairs={{0,12},{2,14},{4,0},{6,2},{8,4},{10,6},{12,8},{14,10},{1,13},{3,15... | collective-permute-start | bytes 393224 | tf_op jit(solution)/shard_map/ppermute | solution.py:33
  142.2 13.9 %collective-permute-start.12 = (bf16[3,256,256]{2,1,0:T(8,128)(2,1)S(1)}, bf16[3,256,256]{2,1,0:T(8,128)(2,1)S(1)}, u32[]{:S(2)}, u32[]{:S(2)}) collective-permute-start(bf16[3,256,256]{2,1,0:T(8,128)(2,1)S(1)} %get-tuple-element.21.three), channel_id=1, source_target_pairs={{0,14},{2,0},{4,2},{6,4},{8,6},{10,8},{12,10},{14,12},{1,15},{3,1}... | collective-permute-start | bytes 1179656 | tf_op jit(solution)/shard_map/ppermute | solution.py:33
  148.1 11.2 %collective-permute-start.11 = (bf16[2,256,256]{2,1,0:T(8,128)(2,1)S(1)}, bf16[2,256,256]{2,1,0:T(8,128)(2,1)S(1)}, u32[]{:S(2)}, u32[]{:S(2)}) collective-permute-start(bf16[2,256,256]{2,1,0:T(8,128)(2,1)S(1)} %get-tuple-element.22), channel_id=1, source_target_pairs={{0,2},{2,4},{4,6},{6,8},{8,10},{10,12},{12,14},{14,0},{1,3},{3,5},... | collective-permute-start | bytes 786440 | tf_op jit(solution)/shard_map/ppermute | solution.py:33
  150.0 14.5 %collective-permute-start.13 = (bf16[3,256,256]{2,1,0:T(8,128)(2,1)S(1)}, bf16[3,256,256]{2,1,0:T(8,128)(2,1)S(1)}, u32[]{:S(2)}, u32[]{:S(2)}) collective-permute-start(bf16[3,256,256]{2,1,0:T(8,128)(2,1)S(1)} %get-tuple-element.21.three), channel_id=1, source_target_pairs={{0,1},{1,0},{2,3},{3,2},{4,5},{5,4},{6,7},{7,6},{8,9},{9,8},{10,11... | collective-permute-start | bytes 1179656 | tf_op jit(solution)/shard_map/ppermute | solution.py:33
  156.1 8.5 %collective-permute-start.15 = (bf16[3,256,256]{2,1,0:T(8,128)(2,1)S(1)}, bf16[3,256,256]{2,1,0:T(8,128)(2,1)S(1)}, u32[]{:S(2)}, u32[]{:S(2)}) collective-permute-start(bf16[3,256,256]{2,1,0:T(8,128)(2,1)S(1)} %collective-permute-done.12.behind), channel_id=1, source_target_pairs={{0,1},{1,0},{2,3},{3,2},{4,5},{5,4},{6,7},{7,6},{8,9},{9,8},{10,11... | collective-permute-start | bytes 1179656 | tf_op jit(solution)/shard_map/ppermute | solution.py:33
  159.4 5.2 %collective-permute-start.14 = (bf16[2,256,256]{2,1,0:T(8,128)(2,1)S(1)}, bf16[2,256,256]{2,1,0:T(8,128)(2,1)S(1)}, u32[]{:S(2)}, u32[]{:S(2)}) collective-permute-start(bf16[2,256,256]{2,1,0:T(8,128)(2,1)S(1)} %collective-permute-done.11.ahead), channel_id=1, source_target_pairs={{0,1},{1,0},{2,3},{3,2},{4,5},{5,4},{6,7},{7,6},{8,9},{9,8},{10,11... | collective-permute-start | bytes 786440 | tf_op jit(solution)/shard_map/ppermute | solution.py:33
  161.9 1.6 copy-start.3
  165.4 6.5 %collective-permute-start.16 = (bf16[32,128]{1,0:T(8,128)(2,1)S(1)}, bf16[32,128]{1,0:T(8,128)(2,1)S(1)}, u32[]{:S(2)}, u32[]{:S(2)}) collective-permute-start(bf16[32,128]{1,0:T(8,128)(2,1)S(1)} %shard_map.101), channel_id=1, source_target_pairs={{0,16},{16,32},{32,48},{48,64},{64,80},{80,96},{96,112},{112,128},... | collective-permute-start | bytes 24584 | tf_op jit(solution)/shard_map/ppermute | solution.py:368
  191.9 7.5 %collective-permute-start.17 = (bf16[8,272,128]{2,1,0:T(8,128)(2,1)S(1)}, bf16[8,272,128]{2,1,0:T(8,128)(2,1)S(1)}, u32[]{:S(2)}, u32[]{:S(2)}) collective-permute-start(bf16[8,272,128]{2,1,0:T(8,128)(2,1)S(1)} %all_to_all.22.own), channel_id=1, source_target_pairs={{0,1},{1,0},{2,3},{3,2},{4,5},{5,4},{6,7},{7,6},{8,9},{9,8},{10,11... | collective-permute-start | bytes 1671176 | tf_op jit(solution)/shard_map/ppermute | solution.py:33
  197.9 1.2 copy-start.4
Sparse Core Ops, SparseCore 0:
  17.0 46.2 all-gather.6
  70.5 45.0 all-gather.8
  159.5 25.5 all-gather.10
where the time goes:
time: 209 us; the launch traced here: 208 us
  starting transfers between devices  71.7 us (34%)
  blocking collectives  62.4 us (30%)
  waiting for transfers between devices  36.5 us (17%)
  Pallas kernels  15.9 us (8%)
  between operations  13.5 us (6%)
  local copies, waits for them, and re-layouts  8.15 us (4%)
    ppermute x16, starting transfers between devices, shifted(): lax.ppermute(x, axis, [(i, (i + steps) % count) for i in range(count)])  63 us
    all_to_all x3, blocking collectives, exchanged(): return lax.all_to_all(x, axis, split_axis=0, concat_axis=0, tiled=True)  62.4 us
    ppermute x16, waiting for transfers between devices, shifted(): lax.ppermute(x, axis, [(i, (i + steps) % count) for i in range(count)])  29.4 us
    unnamed x25, local copies, waits for them, and re-layouts  6.47 us
  transfers between devices with their start and end apart: 22, of which 10 were waited for; matrix products, arithmetic and copies ran while one was open for 0% of the time, Pallas kernels for 5%

commit v1 on v0

v1 whole, which is shorter than its diff:
```python
import functools

import jax
import jax.numpy as jnp
from jax import lax
from jax.experimental import pallas as pl
from jax.experimental.pallas import tpu as pltpu
from jax.sharding import Mesh, PartitionSpec as P


F32 = jnp.float32
BF16 = jnp.bfloat16
HALO = 32
FROM = ((0, 3, -2), (1, 4), (-1, 2, -3))
HBM = pl.BlockSpec(memory_space=pltpu.HBM)
VMEM = pl.BlockSpec(memory_space=pltpu.VMEM)
SMEM = pl.BlockSpec(memory_space=pltpu.SMEM)


def parts_of(x):
    high = x.astype(BF16).astype(F32)
    rest = x - high
    middle = rest.astype(BF16).astype(F32)
    return high, middle, (rest - middle).astype(BF16).astype(F32)


def exchanged(x, axis):
    return lax.all_to_all(x, axis, split_axis=0, concat_axis=0, tiled=True)


def shifted(x, axis, steps):
    count = lax.axis_size(axis)
    return lax.ppermute(x, axis, [(i, (i + steps) % count) for i in range(count)])


def row_dot(ones, x):
    return lax.dot_general(
        ones, x, (((1,), (1,)), ((), ())), precision=lax.Precision.HIGHEST, preferred_element_type=F32
    )


def pack_weights(value, gate, out_weights, first, rest):
    deep, depth = value.shape[1], out_weights.shape[1]
    for copy in range(first.shape[0]):
        first[copy, :, :128] = value[0]
        first[copy, :, 128:] = gate[0]
    rest[:deep, :128] = value[1]
    rest[:deep, 128:] = gate[1]
    rest[deep : deep + depth, :] = out_weights[1]
    rest[deep + depth :, :] = out_weights[0]


def group_kernel(own, third, second, *outs):
    start = 0
    for two, three in zip(outs[::2], outs[1::2], strict=True):
        rows = slice(start, start + two.shape[1])
        for out in (two, three):
            out[0] = own[rows, :]
            out[1] = third[rows, :]
        three[2] = second[rows, :]
        start += two.shape[1]


def pack_tokens(tokens, gains, biases, out, near_gains, near_biases, done):
    rows = tokens.shape[0]
    moves = [
        pltpu.make_async_copy(tokens, out.at[pl.ds(0, rows), :], done.at[0]),
        pltpu.make_async_copy(gains, near_gains, done.at[1]),
        pltpu.make_async_copy(biases, near_biases, done.at[2]),
    ]
    for move in moves:
        move.start()
    at = lax.broadcasted_iota(jnp.int32, (16, 256), 0)
    tile = jnp.zeros((16, 256), F32)
    for move in moves:
        move.wait()
    for layer in range(2):
        pair = jnp.concatenate([near_gains[layer : layer + 1, :], near_biases[layer : layer + 1, :]], axis=1)
        for j, part in enumerate(parts_of(pair)):
            tile = jnp.where(at == 3 * layer + j, part, tile)
    out[rows:, :] = tile.astype(BF16)


def stack_kernel(parts, place, three, ahead, behind, *outs):
    for group, steps in zip((three, ahead, behind), FROM, strict=True):
        for j, step in enumerate(steps):
            z = lax.rem(place[2] + 8 - step, 8)
            for (start, stop), out in zip(parts, outs, strict=True):
                out[z] = group[j, start:stop, :]


def join_gathered(weights, joined):
    depth = weights.shape[2]
    for c in range(2):
        for h in range(2):
            for y in range(weights.shape[1]):
                joined[c, y, h * depth : (h + 1) * depth, :] = weights[2 * c + h, y]


def copy_kernel(x, out, done):
    moves = [pltpu.make_async_copy(x, out.at[copy], done.at[copy]) for copy in range(out.shape[0])]
    for move in moves:
        move.start()
    for move in moves:
        move.wait()


def convolve_and_pack(extended, taps, bias, layer, out, rows):
    kernel = taps.shape[1]
    convolved = jnp.zeros((rows, 128), F32) + bias[layer : layer + 1, :]
    for k in range(kernel):
        convolved = convolved + taps[layer, k : k + 1, :] * extended[pl.ds(HALO - kernel + 1 + k, rows), :]
    mean = jnp.sum(convolved, axis=1, keepdims=True) * (1.0 / 128.0)
    less = convolved - mean
    ones = jnp.ones((8, 128), F32)
    mean_row = row_dot(ones, convolved) * (1.0 / 128.0)
    square_row = row_dot(ones, less * less)
    at = lax.broadcasted_iota(jnp.int32, (8, 128), 0)
    packed = []
    for row in (mean_row, square_row):
        tile = jnp.zeros((8, 128), F32)
        for j, part in enumerate(parts_of(row)):
            for half in range(2):
                tile = jnp.where(at == 2 * j + half, part[:, half * 128 : half * 128 + 128], tile)
        packed.append(tile)
    small = jnp.concatenate(packed, axis=0).astype(BF16)
    less = less.astype(BF16)
    for copy in range(out.shape[0]):
        out[copy, :rows, :] = less
        out[copy, rows:, :] = small


def gated_from(acc, squares, total):
    scale = lax.rsqrt(jnp.sum(squares, axis=1, keepdims=True) / total + 1e-06)
    value = acc[:, :128] * scale
    gate = acc[:, 128:] * scale
    return value * jax.nn.sigmoid(gate)


def first_gate(tokens, gains, weights, out, acc, squares):
    rows = out.shape[0]
    acc[...] = jnp.zeros(acc.shape, F32)
    squares[...] = jnp.zeros(squares.shape, F32)
    for i in range(tokens.shape[0]):
        y, c = divmod(i, 2)
        gain = gains[0:1, i * 256 : i * 256 + 256]
        depths = jnp.concatenate([weights[2 * c, y], weights[2 * c + 1, y]], axis=0)
        product_step(tokens[i, :rows, :], gain, depths, acc, squares)
    out[...] = gated_from(acc, squares[...], tokens.shape[0] * tokens.shape[2]).astype(BF16)


def product_step(block, gain, weights, acc, squares):
    wide = block.astype(F32)
    normed = (wide * gain).astype(BF16)
    wide = wide * wide
    squares[...] += wide[:, :128] + wide[:, 128:]
    acc[...] += jnp.dot(normed, weights, preferred_element_type=F32)


def gate_blocks(blocks, c, first, gains, weights, acc, squares):
    for y in range(blocks.shape[0]):
        gain = gains[1:2, pl.ds(pl.multiple_of((2 * y + c) * 256, 256), 256)]
        depths = jnp.concatenate([weights[2 * c, y], weights[2 * c + 1, y]], axis=0)
        product_step(blocks[y, first:, :], gain, depths, acc, squares)


def gate_own(place, own, gains, weights, acc, squares):
    acc[...] = jnp.zeros(acc.shape, F32)
    squares[...] = jnp.zeros(squares.shape, F32)
    gate_blocks(own, place[0], 0, gains, weights, acc, squares)


def gate_other(place, own_acc, own_squares, other, gains, weights, out, acc, squares):
    first = own_acc.shape[0] - out.shape[0]
    acc[...] = own_acc[first:, :]
    squares[...] = own_squares[first:, :]
    gate_blocks(other, 1 - place[0], first, gains, weights, acc, squares)
    out[...] = gated_from(acc, squares[...], 2 * other.shape[0] * other.shape[2]).astype(BF16)


def conv_kernel(rows, layer, earlier, gated, taps, bias, out, extended):
    extended[:HALO, :] = earlier[...].astype(F32)
    extended[HALO:, :] = gated[...].astype(F32)
    convolve_and_pack(extended, taps, bias, layer, out, rows)


def out_kernel(rows, layer, place, own, other, params, stream, joined, out, acc, sides):
    core = place[0]
    count = own.shape[0]
    total = 2 * count * 128

    def stat(tile):
        sums = []
        for half in range(2):
            sums.append(sum(tile[2 * j + half : 2 * j + half + 1, :] for j in range(3)))
        return jnp.concatenate(sums, axis=1)

    means, squares = [], []
    for blocks in (own, other):
        for y in range(count):
            tile = blocks[y, rows:, :].astype(F32)
            means.append(stat(tile[:8]))
            squares.append(stat(tile[8:]))
    means = jnp.concatenate(means, axis=0)
    squares = jnp.concatenate(squares, axis=0)
    center = jnp.mean(means, axis=0, keepdims=True)
    apart = means - center
    spread = jnp.sum(squares + 128.0 * apart * apart, axis=0, keepdims=True) / total
    factor = lax.rsqrt(spread + 1e-05)
    lines = jnp.concatenate([apart * factor, factor, jnp.zeros((128 - 2 * count - 1, rows), F32)], axis=0)
    sides[...] = lines.T

    acc[...] = stream[...].astype(F32)
    wide = jnp.broadcast_to(sides[:, 2 * count : 2 * count + 1], (rows, 128))
    for n, (blocks, c) in enumerate(((own, core), (other, 1 - core))):
        for y in range(count):
            param = params[2 * y + c].astype(F32)
            gain, bias = (
                sum(param[3 * layer + j : 3 * layer + j + 1, k * 128 : k * 128 + 128] for j in range(3))
                for k in range(2)
            )
            side = sides[:, n * count + y : n * count + y + 1]
            shaped = (blocks[y, :rows, :].astype(F32) * wide + side) * gain + bias
            activated = (shaped * jax.nn.sigmoid(shaped)).astype(BF16)
            acc[...] += jnp.dot(activated, joined[c, y], preferred_element_type=F32)
    result = acc[...].astype(BF16)
    if len(out.shape) == 2:
        out[...] = result
    else:
        for copy in range(out.shape[0]):
            out[copy] = result


def call(body, shape, arrays, scratch=(), scalars=0, flops=1_000_000_000, limit=8, into=VMEM):
    specs = [VMEM] * arrays if isinstance(arrays, int) else arrays
    return pl.pallas_call(
        body,
        out_shape=shape,
        in_specs=[SMEM] * scalars + specs,
        out_specs=jax.tree.map(lambda _: into, shape),
        scratch_shapes=list(scratch),
        cost_estimate=pl.CostEstimate(flops=flops, bytes_accessed=1_000_000, transcendentals=0),
        compiler_params=pltpu.CompilerParams(vmem_limit_bytes=limit * 1024 * 1024),
    )


def shards(tokens, norm_gain, w_value, w_gate, conv_taps, conv_bias, chan_gain, chan_bias, w_out):
    rows, width = tokens.shape
    ring, deep_ring = lax.axis_size("y"), lax.axis_size("z")
    place = jnp.stack([lax.axis_index(axis).astype(jnp.int32) for axis in ("c", "x", "z", "y")])
    blocks = deep_ring * lax.axis_size("x")
    onward = [(i, i + 1) for i in range(blocks - 1)]
    deep, depth = w_value.shape[1], w_out.shape[1]

    packed = call(
        pack_tokens,
        jax.ShapeDtypeStruct((rows + 16, width), BF16),
        [HBM, HBM, HBM],
        scratch=[
            pltpu.VMEM(chan_gain.shape, F32),
            pltpu.VMEM(chan_bias.shape, F32),
            pltpu.SemaphoreType.DMA((3,)),
        ],
        limit=60,
    )(tokens, chan_gain, chan_bias)
    everything = lax.all_gather(packed, ("y", "c"))
    params = everything[:, rows:]

    def relay(x, axis, cuts):
        third, second = shifted(x, axis, 3), shifted(x, axis, -2)
        shapes = [jax.ShapeDtypeStruct((count, cut, width), BF16) for cut in cuts for count in (2, 3)]
        grouped = call(group_kernel, shapes, 3)(x, third, second)
        groups = []
        for two, three in zip(grouped[::2], grouped[1::2], strict=True):
            groups.append((three, shifted(two, axis, 1), shifted(three, axis, -1)))
        return groups

    first, rest = call(
        pack_weights,
        (jax.ShapeDtypeStruct((deep_ring, deep, width), BF16), jax.ShapeDtypeStruct((deep + 2 * depth, width), BF16)),
        3,
    )(w_value, w_gate, w_out)
    first = exchanged(first, "z")
    across = lax.axis_size("x")
    in_first = call(
        copy_kernel,
        jax.ShapeDtypeStruct((across, deep_ring, deep, width), BF16),
        1,
        scratch=[pltpu.SemaphoreType.DMA((across,))],
        into=HBM,
    )(first)
    in_first = exchanged(in_first, "x")
    late, soon = relay(rest, "z", (deep + depth, depth))

    def stacked(groups, *parts):
        shapes = [jax.ShapeDtypeStruct((deep_ring, stop - start, width), BF16) for start, stop in parts]
        return call(functools.partial(stack_kernel, parts), shapes, 3, scalars=1)(place, *groups)

    (out_first,) = stacked(soon, (0, depth))
    in_second, out_second = stacked(late, (0, deep), (deep, deep + depth))
    out_first = lax.all_gather(out_first, "x")
    in_second = lax.all_gather(in_second, "x")
    out_second = lax.all_gather(out_second, "x")

    def convolved(layer, last, gated):
        earlier = lax.ppermute(last, ("z", "x"), onward)
        return call(
            functools.partial(conv_kernel, rows, layer),
            jax.ShapeDtypeStruct((ring, rows + 16, 128), BF16),
            4,
            scratch=[pltpu.VMEM((HALO + rows, 128), F32)],
        )(earlier, gated, conv_taps, conv_bias)

    def gate(count, body, *arrays, scalars=0):
        return call(
            body,
            jax.ShapeDtypeStruct((count, 128), BF16),
            len(arrays) - scalars,
            scratch=[pltpu.VMEM((count, 256), F32), pltpu.VMEM((count, 128), F32)],
            scalars=scalars,
            flops=4_000_000_000,
        )(*arrays)

    def out_step(own, other, stream, layer, weights, copies):
        joined = call(join_gathered, jax.ShapeDtypeStruct((2, ring, 2 * depth, width), BF16), 1)(weights)
        return call(
            functools.partial(out_kernel, rows, layer),
            jax.ShapeDtypeStruct((copies, rows, width) if copies else (rows, width), BF16),
            5,
            scratch=[pltpu.VMEM((rows, width), F32), pltpu.VMEM((rows, 128), F32)],
            scalars=1,
            flops=4_000_000_000,
        )(place, own, other, params, stream, joined)

    tail = everything[:, rows - HALO : rows]
    last = gate(HALO, first_gate, tail, norm_gain, in_first)
    gated = gate(rows, first_gate, everything, norm_gain, in_first)
    packed = convolved(0, last, gated)
    own = exchanged(packed, "y")
    other = shifted(own, "c", 1)
    copies = out_step(own, other, tokens, 0, out_first, ring)
    own = exchanged(copies, "y")
    other = shifted(own, "c", 1)
    sums = (jax.ShapeDtypeStruct((rows, 256), F32), jax.ShapeDtypeStruct((rows, 128), F32))
    acc, squares = call(gate_own, sums, 3, scalars=1, flops=4_000_000_000)(place, own, norm_gain, in_second)

    rest = (place, acc, squares, other, norm_gain, in_second)
    last = gate(HALO, gate_other, *rest, scalars=1)
    gated = gate(rows, gate_other, *rest, scalars=1)
    packed = convolved(1, last, gated)
    own = exchanged(packed, "y")
    other = shifted(own, "c", 1)
    return out_step(own, other, copies[0], 1, out_second, 0)


def solution(mesh):
    grid = Mesh(mesh.devices.reshape(8, 4, 8, 2), ("z", "x", "y", "c"))
    sp, tp = ("z", "x"), ("y", "c")
    placed = (
        P(sp, tp),
        P(),
        P(None, sp, tp),
        P(None, sp, tp),
        P(None, None, tp),
        P(None, tp),
        P(None, tp),
        P(None, tp),
        P(None, sp, tp),
    )
    return jax.shard_map(shards, mesh=grid, in_specs=placed, out_specs=P(sp, tp), check_vma=False)
```

time: 209 us -> 193 us (0.923)
  starting transfers between devices: 71.7 us -> 51.9 us
  blocking collectives: 62.4 us -> 72.1 us
  waiting for transfers between devices: 36.5 us -> 32.2 us
    ppermute x16 -> x9, starting transfers between devices: 63 us -> 34.9 us  [shifted(): lax.ppermute(x, axis, [(i, (i + steps) % count) for i in range(count)])]
    ppermute x16 -> x9, waiting for transfers between devices: 29.4 us -> 15 us  [shifted(): lax.ppermute(x, axis, [(i, (i + steps) % count) for i in range(count)])]
    all_to_all x1 -> x2, waiting for transfers between devices: 0.01 us -> 10.6 us  [exchanged(): return lax.all_to_all(x, axis, split_axis=0, concat_axis=0, tiled=True)]
    all_to_all x3, blocking collectives: 62.4 us -> 72.1 us  [exchanged(): return lax.all_to_all(x, axis, split_axis=0, concat_axis=0, tiled=True)]
    all_to_all x1 -> x2, starting transfers between devices: 3.63 us -> 11 us  [exchanged(): return lax.all_to_all(x, axis, split_axis=0, concat_axis=0, tiled=True)]
    pallas_call x14 -> x16, Pallas kernels: 15.9 us -> 15.3 us  [the longest x2 4.05 us: out_step(): call(functools.partial(out_kernel, rows, layer), jax.ShapeDtypeStruct((co...]
  transfers between devices with their start and end apart: 22 -> 17, of which waited for: 10 -> 8; matrix products, arithmetic and copies ran while one was open for 0% -> 1% of each run, Pallas kernels for 5% -> 6%
where the time goes in v1:
time: 193 us; the launch traced here: 192 us
  blocking collectives  72.1 us (37%)
  starting transfers between devices  51.9 us (27%)
  waiting for transfers between devices  32.2 us (17%)
  Pallas kernels  15.4 us (8%)
  between operations  13.5 us (7%)
  local copies, waits for them, and re-layouts  7.28 us (4%)
    all_to_all x3, blocking collectives, exchanged(): return lax.all_to_all(x, axis, split_axis=0, concat_axis=0, tiled=True)  72.1 us
    ppermute x9, starting transfers between devices, shifted(): lax.ppermute(x, axis, [(i, (i + steps) % count) for i in range(count)])  34.9 us
    ppermute x9, waiting for transfers between devices, shifted(): lax.ppermute(x, axis, [(i, (i + steps) % count) for i in range(count)])  15 us
    all_to_all x2, starting transfers between devices, exchanged(): return lax.all_to_all(x, axis, split_axis=0, concat_axis=0, tiled=True)  11 us
    all_to_all x2, waiting for transfers between devices, exchanged(): return lax.all_to_all(x, axis, split_axis=0, concat_axis=0, tiled=True)  10.6 us
    ppermute x2, waiting for transfers between devices, convolved(): earlier = lax.ppermute(last, ('z', 'x'), onward)  6.44 us
    ppermute x2, starting transfers between devices, convolved(): earlier = lax.ppermute(last, ('z', 'x'), onward)  5.95 us
    unnamed x25, local copies, waits for them, and re-layouts  5.38 us
  transfers between devices with their start and end apart: 17, of which 8 were waited for; matrix products, arithmetic and copies ran while one was open for 1% of the time, Pallas kernels for 6%

profile of v1, /device:TPU:65, one launch (start us, length us, event | category | flops | bytes accessed | tf_op | source)
XLA Modules:
  0.0 192.3 jit_solution(10515321425574278288)
XLA Ops:
  6.5 1.7 shard_map.91
  8.2 0.0 all-gather.9.cloned.1.call-update
  8.3 0.1 shard_map.92
  8.4 23.5 %all_to_all.25.x = bf16[8,128,256]{2,1,0:T(8,128)(2,1)S(1)} all-to-all(bf16[8,128,256]{2,1,0:T(8,128)(2,1)S(1)} %get-tuple-element.15), channel_id=1, replica_groups=mesh['z'=8,'x'=4,'y'=8,'c'=2] {'z'}, dimensions={0} | all-to-all | bytes 1048576 | tf_op jit(solution)/shard_map/all_to_all | solution.py:28
  31.8 0.2 shard_map.93
  32.0 1.3 copy-done
  33.4 4.1 %all-to-all-start.1 = ((bf16[4,8,128,256]{3,2,1,0:T(8,128)(2,1)}), bf16[4,8,128,256]{3,2,1,0:T(8,128)(2,1)S(1)}, u32[]{:S(2)}, u32[]{:S(2)}) async-start(bf16[4,8,128,256]{3,2,1,0:T(8,128)(2,1)} %copy-done), calls=%async_computation.1 | async-start | bytes 4194304 | tf_op jit(solution)/shard_map/all_to_all | solution.py:28
  37.5 3.7 %collective-permute-start.2 = (bf16[256,256]{1,0:T(8,128)(2,1)S(1)}, bf16[256,256]{1,0:T(8,128)(2,1)S(1)}, u32[]{:S(2)}, u32[]{:S(2)}) collective-permute-start(bf16[256,256]{1,0:T(8,128)(2,1)S(1)} %get-tuple-element.16.own), channel_id=1, source_target_pairs={{0,192},{64,256},{128,320},{192,384},{256,448},{320,0},{384,64},{4... | collective-permute-start | bytes 393224 | tf_op jit(solution)/shard_map/ppermute | solution.py:33
  41.2 3.3 %collective-permute-start.3 = (bf16[256,256]{1,0:T(8,128)(2,1)S(1)}, bf16[256,256]{1,0:T(8,128)(2,1)S(1)}, u32[]{:S(2)}, u32[]{:S(2)}) collective-permute-start(bf16[256,256]{1,0:T(8,128)(2,1)S(1)} %get-tuple-element.16.own), channel_id=1, source_target_pairs={{0,384},{64,448},{128,0},{192,64},{256,128},{320,192},{384,256},{4... | collective-permute-start | bytes 393224 | tf_op jit(solution)/shard_map/ppermute | solution.py:33
  44.6 3.9 %collective-permute-done.2.third = bf16[256,256]{1,0:T(8,128)(2,1)S(1)} collective-permute-done((bf16[256,256]{1,0:T(8,128)(2,1)S(1)}, bf16[256,256]{1,0:T(8,128)(2,1)S(1)}, u32[]{:S(2)}, u32[]{:S(2)}) %collective-permute-start.2) | collective-permute-done | bytes 131104 | tf_op jit(solution)/shard_map/ppermute | solution.py:33
  48.5 1.5 collective-permute-done.3.second
  50.1 2.2 %collective-permute-start.5 = (bf16[3,64,256]{2,1,0:T(8,128)(2,1)S(1)}, bf16[3,64,256]{2,1,0:T(8,128)(2,1)S(1)}, u32[]{:S(2)}, u32[]{:S(2)}) collective-permute-start(bf16[3,64,256]{2,1,0:T(8,128)(2,1)S(1)} %get-tuple-element.17.three), channel_id=1, source_target_pairs={{0,448},{64,0},{128,64},{192,128},{256,192},{320,256},{384,320},{4... | collective-permute-start | bytes 294920 | tf_op jit(solution)/shard_map/ppermute | solution.py:33
  52.2 3.1 %collective-permute-start.4 = (bf16[2,64,256]{2,1,0:T(8,128)(2,1)S(1)}, bf16[2,64,256]{2,1,0:T(8,128)(2,1)S(1)}, u32[]{:S(2)}, u32[]{:S(2)}) collective-permute-start(bf16[2,64,256]{2,1,0:T(8,128)(2,1)S(1)} %get-tuple-element.18), channel_id=1, source_target_pairs={{0,64},{64,128},{128,192},{192,256},{256,320},{320,384},{384,448},... | collective-permute-start | bytes 196616 | tf_op jit(solution)/shard_map/ppermute | solution.py:33
  55.4 0.1 pad_add_fusion.place
  55.4 2.9 %collective-permute-done.4.ahead = bf16[2,64,256]{2,1,0:T(8,128)(2,1)S(1)} collective-permute-done((bf16[2,64,256]{2,1,0:T(8,128)(2,1)S(1)}, bf16[2,64,256]{2,1,0:T(8,128)(2,1)S(1)}, u32[]{:S(2)}, u32[]{:S(2)}) %collective-permute-start.4) | collective-permute-done | bytes 65568 | tf_op jit(solution)/shard_map/ppermute | solution.py:33
  58.4 0.0 collective-permute-done.5.behind
  58.4 1.3 shard_map.98
  59.6 0.0 all-gather.11.cloned.1.call-update
  59.7 0.0 all-gather.9.cloned.1.call-done
  59.7 1.0 slice.12.tokens
  60.7 0.0 all-to-all-done.1.weights
  60.7 0.5 shard_map.94
  61.2 0.0 copy-start.10
  61.2 4.0 %collective-permute-start = (bf16[32,128]{1,0:T(8,128)(2,1)S(1)}, bf16[32,128]{1,0:T(8,128)(2,1)S(1)}, u32[]{:S(2)}, u32[]{:S(2)}) collective-permute-start(bf16[32,128]{1,0:T(8,128)(2,1)S(1)} %shard_map.94), channel_id=1, source_target_pairs={{0,16},{16,32},{32,48},{48,64},{64,80},{80,96},{96,112},{112,128},... | collective-permute-start | bytes 24584 | tf_op jit(solution)/shard_map/ppermute | solution.py:306
  65.2 0.0 copy-done.1
  65.2 0.8 shard_map.95.gated
  66.0 2.9 %collective-permute-done.earlier = bf16[32,128]{1,0:T(8,128)(2,1)S(1)} collective-permute-done((bf16[32,128]{1,0:T(8,128)(2,1)S(1)}, bf16[32,128]{1,0:T(8,128)(2,1)S(1)}, u32[]{:S(2)}, u32[]{:S(2)}) %collective-permute-start) | collective-permute-done | bytes 8224 | tf_op jit(solution)/shard_map/ppermute | solution.py:306
  68.9 1.5 shard_map.96
  70.5 6.8 %all-to-all-start.2 = ((bf16[8,272,128]{2,1,0:T(8,128)(2,1)}), bf16[8,272,128]{2,1,0:T(8,128)(2,1)S(1)}, u32[]{:S(2)}, u32[]{:S(2)}) async-start(bf16[8,272,128]{2,1,0:T(8,128)(2,1)} %shard_map.96), calls=%async_computation.2 | async-start | bytes 1114112 | tf_op jit(solution)/shard_map/all_to_all | solution.py:28
  77.3 0.0 all-gather.13.cloned.1.call-start
  77.3 1.9 collective-permute-start.7
  79.3 10.6 %all-to-all-done.2.own = bf16[8,272,128]{2,1,0:T(8,128)(2,1)S(1)} async-done(((bf16[8,272,128]{2,1,0:T(8,128)(2,1)}), bf16[8,272,128]{2,1,0:T(8,128)(2,1)S(1)}, u32[]{:S(2)}, u32[]{:S(2)}) %all-to-all-start.2) | async-done | bytes 557088 | tf_op jit(solution)/shard_map/all_to_all | solution.py:28
  89.9 9.9 %collective-permute-start.1 = (bf16[8,272,128]{2,1,0:T(8,128)(2,1)S(1)}, bf16[8,272,128]{2,1,0:T(8,128)(2,1)S(1)}, u32[]{:S(2)}, u32[]{:S(2)}) collective-permute-start(bf16[8,272,128]{2,1,0:T(8,128)(2,1)S(1)} %all-to-all-done.2.own), channel_id=1, source_target_pairs={{0,1},{1,0},{2,3},{3,2},{4,5},{5,4},{6,7},{7,6},{8,9},{9,8},{10,11... | collective-permute-start | bytes 1671176 | tf_op jit(solution)/shard_map/ppermute | solution.py:33
  99.8 1.9 collective-permute-start.6
  101.7 6.4 %collective-permute-done.6.ahead = bf16[2,192,256]{2,1,0:T(8,128)(2,1)S(1)} collective-permute-done((bf16[2,192,256]{2,1,0:T(8,128)(2,1)S(1)}, bf16[2,192,256]{2,1,0:T(8,128)(2,1)S(1)}, u32[]{:S(2)}, u32[]{:S(2)}) %collective-permute-start.6) | collective-permute-done | bytes 196640 | tf_op jit(solution)/shard_map/ppermute | solution.py:33
  108.1 0.0 collective-permute-done.7.behind
  108.1 1.5 shard_map.101
  109.7 0.0 all-gather.13.cloned.1.call-update
  109.7 0.0 all-gather.15.cloned.1.call-start
  109.7 0.0 all-gather.11.cloned.1.call-done
  109.8 1.2 copy-done.3
  111.0 0.1 shard_map.99.joined
  111.1 0.9 slice.13.params
  112.0 0.0 collective-permute-done.1.other
  112.0 1.7 shard_map.100
  113.7 29.9 %all_to_all.26.own = bf16[8,256,256]{2,1,0:T(8,128)(2,1)S(1)} all-to-all(bf16[8,256,256]{2,1,0:T(8,128)(2,1)S(1)} %shard_map.100), channel_id=1, replica_groups=mesh['z'=8,'x'=4,'y'=8,'c'=2] {'y'}, dimensions={0} | all-to-all | bytes 2097152 | tf_op jit(solution)/shard_map/all_to_all | solution.py:28
  143.6 4.1 %collective-permute-start.8 = (bf16[8,256,256]{2,1,0:T(8,128)(2,1)S(1)}, bf16[8,256,256]{2,1,0:T(8,128)(2,1)S(1)}, u32[]{:S(2)}, u32[]{:S(2)}) collective-permute-start(bf16[8,256,256]{2,1,0:T(8,128)(2,1)S(1)} %all_to_all.26.own), channel_id=1, source_target_pairs={{0,1},{1,0},{2,3},{3,2},{4,5},{5,4},{6,7},{7,6},{8,9},{9,8},{10,11... | collective-permute-start | bytes 3145736 | tf_op jit(solution)/shard_map/ppermute | solution.py:33
  147.7 0.0 all-gather.15.cloned.1.call-update
  147.7 0.0 all-gather.13.cloned.1.call-done
  147.8 1.6 copy-done.2
  149.4 1.0 shard_map.102
  150.4 0.0 collective-permute-done.8.other
  150.4 0.8 shard_map.103
  151.2 1.9 collective-permute-start.9
  153.2 1.1 shard_map.104.gated
  154.2 3.5 %collective-permute-done.9.earlier = bf16[32,128]{1,0:T(8,128)(2,1)S(1)} collective-permute-done((bf16[32,128]{1,0:T(8,128)(2,1)S(1)}, bf16[32,128]{1,0:T(8,128)(2,1)S(1)}, u32[]{:S(2)}, u32[]{:S(2)}) %collective-permute-start.9) | collective-permute-done | bytes 8224 | tf_op jit(solution)/shard_map/ppermute | solution.py:306
  157.7 0.7 shard_map.105
  158.5 18.7 %all_to_all.27.own = bf16[8,272,128]{2,1,0:T(8,128)(2,1)S(1)} all-to-all(bf16[8,272,128]{2,1,0:T(8,128)(2,1)S(1)} %shard_map.105), channel_id=1, replica_groups=mesh['z'=8,'x'=4,'y'=8,'c'=2] {'y'}, dimensions={0} | all-to-all | bytes 1114112 | tf_op jit(solution)/shard_map/all_to_all | solution.py:28
  177.2 4.7 %collective-permute-start.10 = (bf16[8,272,128]{2,1,0:T(8,128)(2,1)S(1)}, bf16[8,272,128]{2,1,0:T(8,128)(2,1)S(1)}, u32[]{:S(2)}, u32[]{:S(2)}) collective-permute-start(bf16[8,272,128]{2,1,0:T(8,128)(2,1)S(1)} %all_to_all.27.own), channel_id=1, source_target_pairs={{0,1},{1,0},{2,3},{3,2},{4,5},{5,4},{6,7},{7,6},{8,9},{9,8},{10,11... | collective-permute-start | bytes 1671176 | tf_op jit(solution)/shard_map/ppermute | solution.py:33
  181.9 0.0 all-gather.15.cloned.1.call-done
  181.9 1.2 copy-done.4
  183.1 0.1 shard_map.106.joined
  183.2 0.2 collective-permute-done.10.other
  183.5 2.4 %shard_map.107 = bf16[256,256]{1,0:T(8,128)(2,1)} custom-call(s32[4]{0:T(128)S(1)} %pad_add_fusion.place, bf16[8,272,128]{2,1,0:T(8,128)(2,1)S(1)} %all_to_all.27.own, bf16[8,272,128]{2,1,0:T(8,128)(2,1)S(1)} %collective-permute-done.10.other, bf16[16,16,256]{2,1,0:T(8,128)(2,1)S(1)} %slice.13.params, bf16[256,256]{1,0:T(8,128)(2,1)S(1)} %slice_bitcast_fusion.stream, ...), custom_call_target="tpu_custom_call" | custom-call | flops 4000000000 | bytes 1000000 | tf_op jit(solution)/shard_map/pallas_call | solution.py:326
  (23 shorter events, 0.1 us)
Async XLA Ops:
  6.5 1.7 copy-start.6
  6.5 1.7 copy-start.7
  6.5 1.7 copy-start.8
  6.5 53.1 %all-gather.9.cloned.1.call-start = ((), (), s32[]{:S(2)}) async-start(), calls=%async_computation.5 | async-start | bytes 2367488 | tf_op jit(solution)/shard_map/all_gather | solution.py:266
  32.0 1.3 copy-start
  33.3 11.2 %copy-start.11 = (f32[2,31,128]{2,0,1:T(2,128)S(1)}, f32[2,31,128]{2,0,1:T(2,128)}, u32[]{:S(2)}) copy-start(f32[2,31,128]{2,0,1:T(2,128)} %param.13) | copy-start | bytes 95236
  33.4 27.3 %all-to-all-start.1 = ((bf16[4,8,128,256]{3,2,1,0:T(8,128)(2,1)}), bf16[4,8,128,256]{3,2,1,0:T(8,128)(2,1)S(1)}, u32[]{:S(2)}, u32[]{:S(2)}) async-start(bf16[4,8,128,256]{3,2,1,0:T(8,128)(2,1)} %copy-done), calls=%async_computation.1 | async-start | bytes 4194304 | tf_op jit(solution)/shard_map/all_to_all | solution.py:28
  37.5 72.3 %all-gather.11.cloned.1.call-start = ((), (), s32[]{:S(2)}) async-start(), calls=%async_computation.6 | async-start | bytes 1310720 | tf_op jit(solution)/shard_map/all_gather | solution.py:301
  37.5 11.0 %collective-permute-start.2 = (bf16[256,256]{1,0:T(8,128)(2,1)S(1)}, bf16[256,256]{1,0:T(8,128)(2,1)S(1)}, u32[]{:S(2)}, u32[]{:S(2)}) collective-permute-start(bf16[256,256]{1,0:T(8,128)(2,1)S(1)} %get-tuple-element.16.own), channel_id=1, source_target_pairs={{0,192},{64,256},{128,320},{192,384},{256,448},{320,0},{384,64},{4... | collective-permute-start | bytes 393224 | tf_op jit(solution)/shard_map/ppermute | solution.py:33
  41.2 8.8 %collective-permute-start.3 = (bf16[256,256]{1,0:T(8,128)(2,1)S(1)}, bf16[256,256]{1,0:T(8,128)(2,1)S(1)}, u32[]{:S(2)}, u32[]{:S(2)}) collective-permute-start(bf16[256,256]{1,0:T(8,128)(2,1)S(1)} %get-tuple-element.16.own), channel_id=1, source_target_pairs={{0,384},{64,448},{128,0},{192,64},{256,128},{320,192},{384,256},{4... | collective-permute-start | bytes 393224 | tf_op jit(solution)/shard_map/ppermute | solution.py:33
  50.1 8.3 %collective-permute-start.5 = (bf16[3,64,256]{2,1,0:T(8,128)(2,1)S(1)}, bf16[3,64,256]{2,1,0:T(8,128)(2,1)S(1)}, u32[]{:S(2)}, u32[]{:S(2)}) collective-permute-start(bf16[3,64,256]{2,1,0:T(8,128)(2,1)S(1)} %get-tuple-element.17.three), channel_id=1, source_target_pairs={{0,448},{64,0},{128,64},{192,128},{256,192},{320,256},{384,320},{4... | collective-permute-start | bytes 294920 | tf_op jit(solution)/shard_map/ppermute | solution.py:33
  52.2 6.1 %collective-permute-start.4 = (bf16[2,64,256]{2,1,0:T(8,128)(2,1)S(1)}, bf16[2,64,256]{2,1,0:T(8,128)(2,1)S(1)}, u32[]{:S(2)}, u32[]{:S(2)}) collective-permute-start(bf16[2,64,256]{2,1,0:T(8,128)(2,1)S(1)} %get-tuple-element.18), channel_id=1, source_target_pairs={{0,64},{64,128},{128,192},{192,256},{256,320},{320,384},{384,448},... | collective-permute-start | bytes 196616 | tf_op jit(solution)/shard_map/ppermute | solution.py:33
  55.4 5.2 %copy-start.9 = (f32[2,4096]{1,0:T(2,128)S(1)}, f32[2,4096]{1,0:T(2,128)}, u32[]{:S(2)}) copy-start(f32[2,4096]{1,0:T(2,128)} %gains.11) | copy-start | bytes 98308
  60.7 4.5 %copy-start.1 = (bf16[4352,256]{1,0:T(8,128)(2,1)S(1)}, bf16[4352,256]{1,0:T(8,128)(2,1)}, u32[]{:S(2)}) copy-start(bf16[4352,256]{1,0:T(8,128)(2,1)} %all-gather.9.cloned.1.call-done) | copy-start | bytes 6684676
  61.2 7.8 %copy-start.10 = (f32[2,128]{1,0:T(2,128)S(1)}, f32[2,128]{1,0:T(2,128)}, u32[]{:S(2)}) copy-start(f32[2,128]{1,0:T(2,128)} %bias.3) | copy-start | bytes 3076
  61.2 7.7 %collective-permute-start = (bf16[32,128]{1,0:T(8,128)(2,1)S(1)}, bf16[32,128]{1,0:T(8,128)(2,1)S(1)}, u32[]{:S(2)}, u32[]{:S(2)}) collective-permute-start(bf16[32,128]{1,0:T(8,128)(2,1)S(1)} %shard_map.94), channel_id=1, source_target_pairs={{0,16},{16,32},{32,48},{48,64},{64,80},{80,96},{96,112},{112,128},... | collective-permute-start | bytes 24584 | tf_op jit(solution)/shard_map/ppermute | solution.py:306
  70.5 19.4 %all-to-all-start.2 = ((bf16[8,272,128]{2,1,0:T(8,128)(2,1)}), bf16[8,272,128]{2,1,0:T(8,128)(2,1)S(1)}, u32[]{:S(2)}, u32[]{:S(2)}) async-start(bf16[8,272,128]{2,1,0:T(8,128)(2,1)} %shard_map.96), calls=%async_computation.2 | async-start | bytes 1114112 | tf_op jit(solution)/shard_map/all_to_all | solution.py:28
  77.3 70.5 %all-gather.13.cloned.1.call-start = ((), (), s32[]{:S(2)}) async-start(), calls=%async_computation.7 | async-start | bytes 2621440 | tf_op jit(solution)/shard_map/all_gather | solution.py:302
  77.3 30.8 %collective-permute-start.7 = (bf16[3,192,256]{2,1,0:T(8,128)(2,1)S(1)}, bf16[3,192,256]{2,1,0:T(8,128)(2,1)S(1)}, u32[]{:S(2)}, u32[]{:S(2)}) collective-permute-start(bf16[3,192,256]{2,1,0:T(8,128)(2,1)S(1)} %get-tuple-element.19.three), channel_id=1, source_target_pairs={{0,448},{64,0},{128,64},{192,128},{256,192},{320,256},{384,320},{4... | collective-permute-start | bytes 884744 | tf_op jit(solution)/shard_map/ppermute | solution.py:33
  89.9 22.1 %collective-permute-start.1 = (bf16[8,272,128]{2,1,0:T(8,128)(2,1)S(1)}, bf16[8,272,128]{2,1,0:T(8,128)(2,1)S(1)}, u32[]{:S(2)}, u32[]{:S(2)}) collective-permute-start(bf16[8,272,128]{2,1,0:T(8,128)(2,1)S(1)} %all-to-all-done.2.own), channel_id=1, source_target_pairs={{0,1},{1,0},{2,3},{3,2},{4,5},{5,4},{6,7},{7,6},{8,9},{9,8},{10,11... | collective-permute-start | bytes 1671176 | tf_op jit(solution)/shard_map/ppermute | solution.py:33
  99.8 8.3 %collective-permute-start.6 = (bf16[2,192,256]{2,1,0:T(8,128)(2,1)S(1)}, bf16[2,192,256]{2,1,0:T(8,128)(2,1)S(1)}, u32[]{:S(2)}, u32[]{:S(2)}) collective-permute-start(bf16[2,192,256]{2,1,0:T(8,128)(2,1)S(1)} %get-tuple-element.20), channel_id=1, source_target_pairs={{0,64},{64,128},{128,192},{192,256},{256,320},{320,384},{384,448},... | collective-permute-start | bytes 589832 | tf_op jit(solution)/shard_map/ppermute | solution.py:33
  109.7 2.3 %copy-start.5 = (bf16[256,256]{1,0:T(8,128)(2,1)S(1)}, bf16[256,256]{1,0:T(8,128)(2,1)}, u32[]{:S(2)}) copy-start(bf16[256,256]{1,0:T(8,128)(2,1)} %stream.1) | copy-start | bytes 393220
  109.7 72.2 %all-gather.15.cloned.1.call-start = ((), (), s32[]{:S(2)}) async-start(), calls=%async_computation.8 | async-start | bytes 1310720 | tf_op jit(solution)/shard_map/all_gather | solution.py:303
  109.8 1.2 copy-start.3
  143.6 6.8 %collective-permute-start.8 = (bf16[8,256,256]{2,1,0:T(8,128)(2,1)S(1)}, bf16[8,256,256]{2,1,0:T(8,128)(2,1)S(1)}, u32[]{:S(2)}, u32[]{:S(2)}) collective-permute-start(bf16[8,256,256]{2,1,0:T(8,128)(2,1)S(1)} %all_to_all.26.own), channel_id=1, source_target_pairs={{0,1},{1,0},{2,3},{3,2},{4,5},{5,4},{6,7},{7,6},{8,9},{9,8},{10,11... | collective-permute-start | bytes 3145736 | tf_op jit(solution)/shard_map/ppermute | solution.py:33
  147.8 1.6 copy-start.2
  151.2 6.5 %collective-permute-start.9 = (bf16[32,128]{1,0:T(8,128)(2,1)S(1)}, bf16[32,128]{1,0:T(8,128)(2,1)S(1)}, u32[]{:S(2)}, u32[]{:S(2)}) collective-permute-start(bf16[32,128]{1,0:T(8,128)(2,1)S(1)} %shard_map.103), channel_id=1, source_target_pairs={{0,16},{16,32},{32,48},{48,64},{64,80},{80,96},{96,112},{112,128},... | collective-permute-start | bytes 24584 | tf_op jit(solution)/shard_map/ppermute | solution.py:306
  177.2 6.3 %collective-permute-start.10 = (bf16[8,272,128]{2,1,0:T(8,128)(2,1)S(1)}, bf16[8,272,128]{2,1,0:T(8,128)(2,1)S(1)}, u32[]{:S(2)}, u32[]{:S(2)}) collective-permute-start(bf16[8,272,128]{2,1,0:T(8,128)(2,1)S(1)} %all_to_all.27.own), channel_id=1, source_target_pairs={{0,1},{1,0},{2,3},{3,2},{4,5},{5,4},{6,7},{7,6},{8,9},{9,8},{10,11... | collective-permute-start | bytes 1671176 | tf_op jit(solution)/shard_map/ppermute | solution.py:33
  181.9 1.2 copy-start.4
Sparse Core Ops, SparseCore 0:
  9.5 46.1 all-gather.8
  59.8 33.1 all-gather.10
  109.8 31.0 all-gather.12
  147.9 22.7 all-gather.14

commit v2 on v1

--- a/solution.py
+++ b/solution.py
@@ -14,7 +14,6 @@
 FROM = ((0, 3, -2), (1, 4), (-1, 2, -3))
 HBM = pl.BlockSpec(memory_space=pltpu.HBM)
 VMEM = pl.BlockSpec(memory_space=pltpu.VMEM)
-SMEM = pl.BlockSpec(memory_space=pltpu.SMEM)
 
 
 def parts_of(x):
@@ -81,10 +80,10 @@
     out[rows:, :] = tile.astype(BF16)
 
 
-def stack_kernel(parts, place, three, ahead, behind, *outs):
+def stack_kernel(parts, three, ahead, behind, *outs):
     for group, steps in zip((three, ahead, behind), FROM, strict=True):
         for j, step in enumerate(steps):
-            z = lax.rem(place[2] + 8 - step, 8)
+            z = lax.rem(lax.axis_index("z") + 8 - step, 8)
             for (start, stop), out in zip(parts, outs, strict=True):
                 out[z] = group[j, start:stop, :]
 
@@ -164,17 +163,17 @@
         product_step(blocks[y, first:, :], gain, depths, acc, squares)
 
 
-def gate_own(place, own, gains, weights, acc, squares):
+def gate_own(own, gains, weights, acc, squares):
     acc[...] = jnp.zeros(acc.shape, F32)
     squares[...] = jnp.zeros(squares.shape, F32)
-    gate_blocks(own, place[0], 0, gains, weights, acc, squares)
-
-
-def gate_other(place, own_acc, own_squares, other, gains, weights, out, acc, squares):
+    gate_blocks(own, lax.axis_index("c"), 0, gains, weights, acc, squares)
+
+
+def gate_other(own_acc, own_squares, other, gains, weights, out, acc, squares):
     first = own_acc.shape[0] - out.shape[0]
     acc[...] = own_acc[first:, :]
     squares[...] = own_squares[first:, :]
-    gate_blocks(other, 1 - place[0], first, gains, weights, acc, squares)
+    gate_blocks(other, 1 - lax.axis_index("c"), first, gains, weights, acc, squares)
     out[...] = gated_from(acc, squares[...], 2 * other.shape[0] * other.shape[2]).astype(BF16)
 
 
@@ -184,8 +183,9 @@
     convolve_and_pack(extended, taps, bias, layer, out, rows)
 
 
-def out_kernel(rows, layer, place, own, other, params, stream, joined, out, acc, sides):
-    core = place[0]
+def out_kernel(rows, layer, own, other, params, stream, joined, *rest):
+    core = lax.axis_index("c")
+    outs, (acts, sides) = rest[:-2], rest[-2:]
     count = own.shape[0]
     total = 2 * count * 128
 
@@ -210,8 +210,8 @@
     lines = jnp.concatenate([apart * factor, factor, jnp.zeros((128 - 2 * count - 1, rows), F32)], axis=0)
     sides[...] = lines.T
 
-    acc[...] = stream[...].astype(F32)
     wide = jnp.broadcast_to(sides[:, 2 * count : 2 * count + 1], (rows, 128))
+    total = stream[...].astype(F32)
     for n, (blocks, c) in enumerate(((own, core), (other, 1 - core))):
         for y in range(count):
             param = params[2 * y + c].astype(F32)
@@ -221,22 +221,22 @@
             )
             side = sides[:, n * count + y : n * count + y + 1]
             shaped = (blocks[y, :rows, :].astype(F32) * wide + side) * gain + bias
-            activated = (shaped * jax.nn.sigmoid(shaped)).astype(BF16)
-            acc[...] += jnp.dot(activated, joined[c, y], preferred_element_type=F32)
-    result = acc[...].astype(BF16)
-    if len(out.shape) == 2:
-        out[...] = result
-    else:
+            acts[:, y * 128 : y * 128 + 128] = (shaped * jax.nn.sigmoid(shaped)).astype(BF16)
+        weights = joined[c].reshape(count * 128, joined.shape[3])
+        total = total + jnp.dot(acts[...], weights, preferred_element_type=F32)
+    result = total.astype(BF16)
+    outs[0][...] = result
+    for out in outs[1:]:
         for copy in range(out.shape[0]):
             out[copy] = result
 
 
-def call(body, shape, arrays, scratch=(), scalars=0, flops=1_000_000_000, limit=8, into=VMEM):
+def call(body, shape, arrays, scratch=(), flops=1_000_000_000, limit=8, into=VMEM):
     specs = [VMEM] * arrays if isinstance(arrays, int) else arrays
     return pl.pallas_call(
         body,
         out_shape=shape,
-        in_specs=[SMEM] * scalars + specs,
+        in_specs=specs,
         out_specs=jax.tree.map(lambda _: into, shape),
         scratch_shapes=list(scratch),
         cost_estimate=pl.CostEstimate(flops=flops, bytes_accessed=1_000_000, transcendentals=0),
@@ -247,7 +247,6 @@
 def shards(tokens, norm_gain, w_value, w_gate, conv_taps, conv_bias, chan_gain, chan_bias, w_out):
     rows, width = tokens.shape
     ring, deep_ring = lax.axis_size("y"), lax.axis_size("z")
-    place = jnp.stack([lax.axis_index(axis).astype(jnp.int32) for axis in ("c", "x", "z", "y")])
     blocks = deep_ring * lax.axis_size("x")
     onward = [(i, i + 1) for i in range(blocks - 1)]
     deep, depth = w_value.shape[1], w_out.shape[1]
@@ -272,7 +271,8 @@
         grouped = call(group_kernel, shapes, 3)(x, third, second)
         groups = []
         for two, three in zip(grouped[::2], grouped[1::2], strict=True):
-            groups.append((three, shifted(two, axis, 1), shifted(three, axis, -1)))
+            behind = shifted(three, axis, -1)
+            groups.append((three, shifted(two, axis, 1), behind))
         return groups
 
     first, rest = call(
@@ -294,10 +294,11 @@
 
     def stacked(groups, *parts):
         shapes = [jax.ShapeDtypeStruct((deep_ring, stop - start, width), BF16) for start, stop in parts]
-        return call(functools.partial(stack_kernel, parts), shapes, 3, scalars=1)(place, *groups)
+        return call(functools.partial(stack_kernel, parts), shapes, 3)(*groups)
 
     (out_first,) = stacked(soon, (0, depth))
-    in_second, out_second = stacked(late, (0, deep), (deep, deep + depth))
+    (in_second,) = stacked(late, (0, deep))
+    (out_second,) = stacked(late, (deep, deep + depth))
     out_first = lax.all_gather(out_first, "x")
     in_second = lax.all_gather(in_second, "x")
     out_second = lax.all_gather(out_second, "x")
@@ -311,13 +312,12 @@
             scratch=[pltpu.VMEM((HALO + rows, 128), F32)],
         )(earlier, gated, conv_taps, conv_bias)
 
-    def gate(count, body, *arrays, scalars=0):
+    def gate(count, body, *arrays):
         return call(
             body,
             jax.ShapeDtypeStruct((count, 128), BF16),
-            len(arrays) - scalars,
+            len(arrays),
             scratch=[pltpu.VMEM((count, 256), F32), pltpu.VMEM((count, 128), F32)],
-            scalars=scalars,
             flops=4_000_000_000,
         )(*arrays)
 
@@ -325,12 +325,11 @@
         joined = call(join_gathered, jax.ShapeDtypeStruct((2, ring, 2 * depth, width), BF16), 1)(weights)
         return call(
             functools.partial(out_kernel, rows, layer),
-            jax.ShapeDtypeStruct((copies, rows, width) if copies else (rows, width), BF16),
+            [jax.ShapeDtypeStruct((*count, rows, width), BF16) for count in ((), (copies,))[: 1 + bool(copies)]],
             5,
-            scratch=[pltpu.VMEM((rows, width), F32), pltpu.VMEM((rows, 128), F32)],
-            scalars=1,
+            scratch=[pltpu.VMEM((rows, ring * 128), BF16), pltpu.VMEM((rows, 128), F32)],
             flops=4_000_000_000,
-        )(place, own, other, params, stream, joined)
+        )(own, other, params, stream, joined)
 
     tail = everything[:, rows - HALO : rows]
     last = gate(HALO, first_gate, tail, norm_gain, in_first)
@@ -338,19 +337,21 @@
     packed = convolved(0, last, gated)
     own = exchanged(packed, "y")
     other = shifted(own, "c", 1)
-    copies = out_step(own, other, tokens, 0, out_first, ring)
+    stream, copies = out_step(own, other, tokens, 0, out_first, ring)
     own = exchanged(copies, "y")
     other = shifted(own, "c", 1)
     sums = (jax.ShapeDtypeStruct((rows, 256), F32), jax.ShapeDtypeStruct((rows, 128), F32))
-    acc, squares = call(gate_own, sums, 3, scalars=1, flops=4_000_000_000)(place, own, norm_gain, in_second)
-
-    rest = (place, acc, squares, other, norm_gain, in_second)
-    last = gate(HALO, gate_other, *rest, scalars=1)
-    gated = gate(rows, gate_other, *rest, scalars=1)
+    acc, squares = call(gate_own, sums, 3, flops=4_000_000_000)(
+        own, norm_gain, in_second
+    )
+
+    rest = (acc, squares, other, norm_gain, in_second)
+    last = gate(HALO, gate_other, *rest)
+    gated = gate(rows, gate_other, *rest)
     packed = convolved(1, last, gated)
     own = exchanged(packed, "y")
     other = shifted(own, "c", 1)
-    return out_step(own, other, copies[0], 1, out_second, 0)
+    return out_step(own, other, stream, 1, out_second, 0)[0]
 
 
 def solution(mesh):

time: 193 us -> 191 us (0.990)
  Pallas kernels: 15.4 us -> 12.3 us
    pallas_call x9 -> x10, Pallas kernels: 11 us -> 7.88 us  [the longest x2 3.02 us: out_step(): call(functools.partial(out_kernel, rows, layer), [jax.ShapeDtypeStruct((*...]
  transfers between devices with their start and end apart: 17 -> 17, of which waited for: 8 -> 9; matrix products, arithmetic and copies ran while one was open for 1% -> 1% of each run, Pallas kernels for 6% -> 5%
where the time goes in v2:
time: 191 us; the launch traced here: 190 us
  blocking collectives  72.1 us (38%)
  starting transfers between devices  51.5 us (27%)
  waiting for transfers between devices  33.2 us (17%)
  between operations  13.5 us (7%)
  Pallas kernels  12.3 us (6%)
  local copies, waits for them, and re-layouts  7.28 us (4%)
    all_to_all x3, blocking collectives, exchanged(): return lax.all_to_all(x, axis, split_axis=0, concat_axis=0, tiled=True)  72.1 us
    ppermute x9, starting transfers between devices, shifted(): lax.ppermute(x, axis, [(i, (i + steps) % count) for i in range(count)])  35 us
    ppermute x9, waiting for transfers between devices, shifted(): lax.ppermute(x, axis, [(i, (i + steps) % count) for i in range(count)])  15.1 us
    all_to_all x2, waiting for transfers between devices, exchanged(): return lax.all_to_all(x, axis, split_axis=0, concat_axis=0, tiled=True)  11 us
    all_to_all x2, starting transfers between devices, exchanged(): return lax.all_to_all(x, axis, split_axis=0, concat_axis=0, tiled=True)  10.8 us
    ppermute x2, waiting for transfers between devices, convolved(): earlier = lax.ppermute(last, ('z', 'x'), onward)  6.99 us
    ppermute x2, starting transfers between devices, convolved(): earlier = lax.ppermute(last, ('z', 'x'), onward)  5.62 us
    unnamed x25, local copies, waits for them, and re-layouts  5.38 us
  transfers between devices with their start and end apart: 17, of which 9 were waited for; matrix products, arithmetic and copies ran while one was open for 1% of the time, Pallas kernels for 5%

profile of v2, /device:TPU:65, one launch (start us, length us, event | category | flops | bytes accessed | tf_op | source)
XLA Modules:
  0.0 189.8 jit_solution(8343413634951765631)
XLA Ops:
  6.5 1.7 shard_map.91
  8.2 0.0 all-gather.9.cloned.1.call-update
  8.3 0.1 shard_map.92
  8.4 23.5 %all_to_all.25.x = bf16[8,128,256]{2,1,0:T(8,128)(2,1)S(1)} all-to-all(bf16[8,128,256]{2,1,0:T(8,128)(2,1)S(1)} %get-tuple-element.15), channel_id=1, replica_groups=mesh['z'=8,'x'=4,'y'=8,'c'=2] {'z'}, dimensions={0} | all-to-all | bytes 1048576 | tf_op jit(solution)/shard_map/all_to_all | solution.py:27
  31.8 0.2 shard_map.93
  32.0 1.3 copy-done
  33.3 4.0 %all-to-all-start.1 = ((bf16[4,8,128,256]{3,2,1,0:T(8,128)(2,1)}), bf16[4,8,128,256]{3,2,1,0:T(8,128)(2,1)S(1)}, u32[]{:S(2)}, u32[]{:S(2)}) async-start(bf16[4,8,128,256]{3,2,1,0:T(8,128)(2,1)} %copy-done), calls=%async_computation.1 | async-start | bytes 4194304 | tf_op jit(solution)/shard_map/all_to_all | solution.py:27
  37.4 3.9 %collective-permute-start.2 = (bf16[256,256]{1,0:T(8,128)(2,1)S(1)}, bf16[256,256]{1,0:T(8,128)(2,1)S(1)}, u32[]{:S(2)}, u32[]{:S(2)}) collective-permute-start(bf16[256,256]{1,0:T(8,128)(2,1)S(1)} %get-tuple-element.16.own), channel_id=1, source_target_pairs={{0,192},{64,256},{128,320},{192,384},{256,448},{320,0},{384,64},{4... | collective-permute-start | bytes 393224 | tf_op jit(solution)/shard_map/ppermute | solution.py:32
  41.2 3.3 %collective-permute-start.3 = (bf16[256,256]{1,0:T(8,128)(2,1)S(1)}, bf16[256,256]{1,0:T(8,128)(2,1)S(1)}, u32[]{:S(2)}, u32[]{:S(2)}) collective-permute-start(bf16[256,256]{1,0:T(8,128)(2,1)S(1)} %get-tuple-element.16.own), channel_id=1, source_target_pairs={{0,384},{64,448},{128,0},{192,64},{256,128},{320,192},{384,256},{4... | collective-permute-start | bytes 393224 | tf_op jit(solution)/shard_map/ppermute | solution.py:32
  44.6 4.0 %collective-permute-done.2.third = bf16[256,256]{1,0:T(8,128)(2,1)S(1)} collective-permute-done((bf16[256,256]{1,0:T(8,128)(2,1)S(1)}, bf16[256,256]{1,0:T(8,128)(2,1)S(1)}, u32[]{:S(2)}, u32[]{:S(2)}) %collective-permute-start.2) | collective-permute-done | bytes 131104 | tf_op jit(solution)/shard_map/ppermute | solution.py:32
  48.5 1.5 collective-permute-done.3.second
  50.1 2.2 %collective-permute-start.5 = (bf16[3,64,256]{2,1,0:T(8,128)(2,1)S(1)}, bf16[3,64,256]{2,1,0:T(8,128)(2,1)S(1)}, u32[]{:S(2)}, u32[]{:S(2)}) collective-permute-start(bf16[3,64,256]{2,1,0:T(8,128)(2,1)S(1)} %get-tuple-element.17.three), channel_id=1, source_target_pairs={{0,448},{64,0},{128,64},{192,128},{256,192},{320,256},{384,320},{4... | collective-permute-start | bytes 294920 | tf_op jit(solution)/shard_map/ppermute | solution.py:32
  52.2 3.1 %collective-permute-start.4 = (bf16[2,64,256]{2,1,0:T(8,128)(2,1)S(1)}, bf16[2,64,256]{2,1,0:T(8,128)(2,1)S(1)}, u32[]{:S(2)}, u32[]{:S(2)}) collective-permute-start(bf16[2,64,256]{2,1,0:T(8,128)(2,1)S(1)} %get-tuple-element.18), channel_id=1, source_target_pairs={{0,64},{64,128},{128,192},{192,256},{256,320},{320,384},{384,448},... | collective-permute-start | bytes 196616 | tf_op jit(solution)/shard_map/ppermute | solution.py:32
  55.4 0.0 copy-start.9
  55.4 3.0 %collective-permute-done.4.ahead = bf16[2,64,256]{2,1,0:T(8,128)(2,1)S(1)} collective-permute-done((bf16[2,64,256]{2,1,0:T(8,128)(2,1)S(1)}, bf16[2,64,256]{2,1,0:T(8,128)(2,1)S(1)}, u32[]{:S(2)}, u32[]{:S(2)}) %collective-permute-start.4) | collective-permute-done | bytes 65568 | tf_op jit(solution)/shard_map/ppermute | solution.py:32
  58.4 0.0 collective-permute-done.5.behind
  58.4 0.7 shard_map.98
  59.1 0.0 all-gather.11.cloned.1.call-update
  59.1 0.0 all-gather.9.cloned.1.call-done
  59.2 1.0 slice.8.tokens
  60.1 0.4 all-to-all-done.1.weights
  60.5 0.5 shard_map.94
  61.0 0.0 copy-start.10
  61.0 3.7 %collective-permute-start = (bf16[32,128]{1,0:T(8,128)(2,1)S(1)}, bf16[32,128]{1,0:T(8,128)(2,1)S(1)}, u32[]{:S(2)}, u32[]{:S(2)}) collective-permute-start(bf16[32,128]{1,0:T(8,128)(2,1)S(1)} %shard_map.94), channel_id=1, source_target_pairs={{0,16},{16,32},{32,48},{48,64},{64,80},{80,96},{96,112},{112,128},... | collective-permute-start | bytes 24584 | tf_op jit(solution)/shard_map/ppermute | solution.py:307
  64.7 0.8 shard_map.95.gated
  65.5 2.9 %collective-permute-done.earlier = bf16[32,128]{1,0:T(8,128)(2,1)S(1)} collective-permute-done((bf16[32,128]{1,0:T(8,128)(2,1)S(1)}, bf16[32,128]{1,0:T(8,128)(2,1)S(1)}, u32[]{:S(2)}, u32[]{:S(2)}) %collective-permute-start) | collective-permute-done | bytes 8224 | tf_op jit(solution)/shard_map/ppermute | solution.py:307
  68.4 1.5 shard_map.96
  69.9 6.8 %all-to-all-start.2 = ((bf16[8,272,128]{2,1,0:T(8,128)(2,1)}), bf16[8,272,128]{2,1,0:T(8,128)(2,1)S(1)}, u32[]{:S(2)}, u32[]{:S(2)}) async-start(bf16[8,272,128]{2,1,0:T(8,128)(2,1)} %shard_map.96), calls=%async_computation.2 | async-start | bytes 1114112 | tf_op jit(solution)/shard_map/all_to_all | solution.py:27
  76.8 0.0 all-gather.13.cloned.1.call-start
  76.8 1.9 %collective-permute-start.7 = (bf16[3,192,256]{2,1,0:T(8,128)(2,1)S(1)}, bf16[3,192,256]{2,1,0:T(8,128)(2,1)S(1)}, u32[]{:S(2)}, u32[]{:S(2)}) collective-permute-start(bf16[3,192,256]{2,1,0:T(8,128)(2,1)S(1)} %get-tuple-element.20.three), channel_id=1, source_target_pairs={{0,448},{64,0},{128,64},{192,128},{256,192},{320,256},{384,320},{4... | collective-permute-start | bytes 884744 | tf_op jit(solution)/shard_map/ppermute | solution.py:32
  78.7 10.6 %all-to-all-done.2.own = bf16[8,272,128]{2,1,0:T(8,128)(2,1)S(1)} async-done(((bf16[8,272,128]{2,1,0:T(8,128)(2,1)}), bf16[8,272,128]{2,1,0:T(8,128)(2,1)S(1)}, u32[]{:S(2)}, u32[]{:S(2)}) %all-to-all-start.2) | async-done | bytes 557088 | tf_op jit(solution)/shard_map/all_to_all | solution.py:27
  89.4 9.9 %collective-permute-start.1 = (bf16[8,272,128]{2,1,0:T(8,128)(2,1)S(1)}, bf16[8,272,128]{2,1,0:T(8,128)(2,1)S(1)}, u32[]{:S(2)}, u32[]{:S(2)}) collective-permute-start(bf16[8,272,128]{2,1,0:T(8,128)(2,1)S(1)} %all-to-all-done.2.own), channel_id=1, source_target_pairs={{0,1},{1,0},{2,3},{3,2},{4,5},{5,4},{6,7},{7,6},{8,9},{9,8},{10,11... | collective-permute-start | bytes 1671176 | tf_op jit(solution)/shard_map/ppermute | solution.py:32
  99.2 1.9 %collective-permute-start.6 = (bf16[2,192,256]{2,1,0:T(8,128)(2,1)S(1)}, bf16[2,192,256]{2,1,0:T(8,128)(2,1)S(1)}, u32[]{:S(2)}, u32[]{:S(2)}) collective-permute-start(bf16[2,192,256]{2,1,0:T(8,128)(2,1)S(1)} %get-tuple-element.21), channel_id=1, source_target_pairs={{0,64},{64,128},{128,192},{192,256},{256,320},{320,384},{384,448},... | collective-permute-start | bytes 589832 | tf_op jit(solution)/shard_map/ppermute | solution.py:32
  101.2 6.4 %collective-permute-done.6.ahead = bf16[2,192,256]{2,1,0:T(8,128)(2,1)S(1)} collective-permute-done((bf16[2,192,256]{2,1,0:T(8,128)(2,1)S(1)}, bf16[2,192,256]{2,1,0:T(8,128)(2,1)S(1)}, u32[]{:S(2)}, u32[]{:S(2)}) %collective-permute-start.6) | collective-permute-done | bytes 196640 | tf_op jit(solution)/shard_map/ppermute | solution.py:32
  107.6 0.0 collective-permute-done.7.behind
  107.6 0.9 shard_map.101
  108.4 0.0 all-gather.13.cloned.1.call-update
  108.5 0.0 all-gather.15.cloned.1.call-start
  108.5 0.0 all-gather.11.cloned.1.call-done
  108.5 1.2 copy-done.3
  109.8 0.1 shard_map.99.joined
  109.8 0.9 slice.9.params
  110.8 0.0 collective-permute-done.1.other
  110.8 1.2 shard_map.100
  112.0 29.9 %all_to_all.26.own = bf16[8,256,256]{2,1,0:T(8,128)(2,1)S(1)} all-to-all(bf16[8,256,256]{2,1,0:T(8,128)(2,1)S(1)} %get-tuple-element.19), channel_id=1, replica_groups=mesh['z'=8,'x'=4,'y'=8,'c'=2] {'y'}, dimensions={0} | all-to-all | bytes 2097152 | tf_op jit(solution)/shard_map/all_to_all | solution.py:27
  141.9 4.1 %collective-permute-start.8 = (bf16[8,256,256]{2,1,0:T(8,128)(2,1)S(1)}, bf16[8,256,256]{2,1,0:T(8,128)(2,1)S(1)}, u32[]{:S(2)}, u32[]{:S(2)}) collective-permute-start(bf16[8,256,256]{2,1,0:T(8,128)(2,1)S(1)} %all_to_all.26.own), channel_id=1, source_target_pairs={{0,1},{1,0},{2,3},{3,2},{4,5},{5,4},{6,7},{7,6},{8,9},{9,8},{10,11... | collective-permute-start | bytes 3145736 | tf_op jit(solution)/shard_map/ppermute | solution.py:32
  146.0 0.7 shard_map.106
  146.7 0.0 all-gather.15.cloned.1.call-update
  146.7 0.0 all-gather.13.cloned.1.call-done
  146.8 1.6 copy-done.2
  148.4 0.5 shard_map.102
  148.9 0.0 collective-permute-done.8.other
  148.9 0.3 shard_map.103
  149.2 1.9 %collective-permute-start.9 = (bf16[32,128]{1,0:T(8,128)(2,1)S(1)}, bf16[32,128]{1,0:T(8,128)(2,1)S(1)}, u32[]{:S(2)}, u32[]{:S(2)}) collective-permute-start(bf16[32,128]{1,0:T(8,128)(2,1)S(1)} %shard_map.103), channel_id=1, source_target_pairs={{0,16},{16,32},{32,48},{48,64},{64,80},{80,96},{96,112},{112,128},... | collective-permute-start | bytes 24584 | tf_op jit(solution)/shard_map/ppermute | solution.py:307
  151.1 0.5 shard_map.104.gated
  151.6 4.1 %collective-permute-done.9.earlier = bf16[32,128]{1,0:T(8,128)(2,1)S(1)} collective-permute-done((bf16[32,128]{1,0:T(8,128)(2,1)S(1)}, bf16[32,128]{1,0:T(8,128)(2,1)S(1)}, u32[]{:S(2)}, u32[]{:S(2)}) %collective-permute-start.9) | collective-permute-done | bytes 8224 | tf_op jit(solution)/shard_map/ppermute | solution.py:307
  155.7 0.7 shard_map.105
  156.4 18.7 %all_to_all.27.own = bf16[8,272,128]{2,1,0:T(8,128)(2,1)S(1)} all-to-all(bf16[8,272,128]{2,1,0:T(8,128)(2,1)S(1)} %shard_map.105), channel_id=1, replica_groups=mesh['z'=8,'x'=4,'y'=8,'c'=2] {'y'}, dimensions={0} | all-to-all | bytes 1114112 | tf_op jit(solution)/shard_map/all_to_all | solution.py:27
  175.1 4.7 %collective-permute-start.10 = (bf16[8,272,128]{2,1,0:T(8,128)(2,1)S(1)}, bf16[8,272,128]{2,1,0:T(8,128)(2,1)S(1)}, u32[]{:S(2)}, u32[]{:S(2)}) collective-permute-start(bf16[8,272,128]{2,1,0:T(8,128)(2,1)S(1)} %all_to_all.27.own), channel_id=1, source_target_pairs={{0,1},{1,0},{2,3},{3,2},{4,5},{5,4},{6,7},{7,6},{8,9},{9,8},{10,11... | collective-permute-start | bytes 1671176 | tf_op jit(solution)/shard_map/ppermute | solution.py:32
  179.8 0.0 all-gather.15.cloned.1.call-done
  179.9 1.2 copy-done.4
  181.1 0.1 shard_map.107.joined
  181.2 0.2 collective-permute-done.10.other
  181.4 1.8 shard_map.108
  (22 shorter events, 0.1 us)
Async XLA Ops:
  6.5 1.7 copy-start.6
  6.5 1.7 copy-start.7
  6.5 1.7 copy-start.8
  6.5 52.6 %all-gather.9.cloned.1.call-start = ((), (), s32[]{:S(2)}) async-start(), calls=%async_computation.5 | async-start | bytes 2367488 | tf_op jit(solution)/shard_map/all_gather | solution.py:265
  32.0 1.3 copy-start
  33.3 27.2 %all-to-all-start.1 = ((bf16[4,8,128,256]{3,2,1,0:T(8,128)(2,1)}), bf16[4,8,128,256]{3,2,1,0:T(8,128)(2,1)S(1)}, u32[]{:S(2)}, u32[]{:S(2)}) async-start(bf16[4,8,128,256]{3,2,1,0:T(8,128)(2,1)} %copy-done), calls=%async_computation.1 | async-start | bytes 4194304 | tf_op jit(solution)/shard_map/all_to_all | solution.py:27
  37.4 18.0 %copy-start.11 = (f32[2,31,128]{2,0,1:T(2,128)S(1)}, f32[2,31,128]{2,0,1:T(2,128)}, u32[]{:S(2)}) copy-start(f32[2,31,128]{2,0,1:T(2,128)} %param.13) | copy-start | bytes 95236
  37.4 71.2 %all-gather.11.cloned.1.call-start = ((), (), s32[]{:S(2)}) async-start(), calls=%async_computation.6 | async-start | bytes 1310720 | tf_op jit(solution)/shard_map/all_gather | solution.py:302
  37.4 11.2 %collective-permute-start.2 = (bf16[256,256]{1,0:T(8,128)(2,1)S(1)}, bf16[256,256]{1,0:T(8,128)(2,1)S(1)}, u32[]{:S(2)}, u32[]{:S(2)}) collective-permute-start(bf16[256,256]{1,0:T(8,128)(2,1)S(1)} %get-tuple-element.16.own), channel_id=1, source_target_pairs={{0,192},{64,256},{128,320},{192,384},{256,448},{320,0},{384,64},{4... | collective-permute-start | bytes 393224 | tf_op jit(solution)/shard_map/ppermute | solution.py:32
  41.2 8.8 %collective-permute-start.3 = (bf16[256,256]{1,0:T(8,128)(2,1)S(1)}, bf16[256,256]{1,0:T(8,128)(2,1)S(1)}, u32[]{:S(2)}, u32[]{:S(2)}) collective-permute-start(bf16[256,256]{1,0:T(8,128)(2,1)S(1)} %get-tuple-element.16.own), channel_id=1, source_target_pairs={{0,384},{64,448},{128,0},{192,64},{256,128},{320,192},{384,256},{4... | collective-permute-start | bytes 393224 | tf_op jit(solution)/shard_map/ppermute | solution.py:32
  50.1 8.3 %collective-permute-start.5 = (bf16[3,64,256]{2,1,0:T(8,128)(2,1)S(1)}, bf16[3,64,256]{2,1,0:T(8,128)(2,1)S(1)}, u32[]{:S(2)}, u32[]{:S(2)}) collective-permute-start(bf16[3,64,256]{2,1,0:T(8,128)(2,1)S(1)} %get-tuple-element.17.three), channel_id=1, source_target_pairs={{0,448},{64,0},{128,64},{192,128},{256,192},{320,256},{384,320},{4... | collective-permute-start | bytes 294920 | tf_op jit(solution)/shard_map/ppermute | solution.py:32
  52.2 6.1 %collective-permute-start.4 = (bf16[2,64,256]{2,1,0:T(8,128)(2,1)S(1)}, bf16[2,64,256]{2,1,0:T(8,128)(2,1)S(1)}, u32[]{:S(2)}, u32[]{:S(2)}) collective-permute-start(bf16[2,64,256]{2,1,0:T(8,128)(2,1)S(1)} %get-tuple-element.18), channel_id=1, source_target_pairs={{0,64},{64,128},{128,192},{192,256},{256,320},{320,384},{384,448},... | collective-permute-start | bytes 196616 | tf_op jit(solution)/shard_map/ppermute | solution.py:32
  55.4 5.1 %copy-start.9 = (f32[2,4096]{1,0:T(2,128)S(1)}, f32[2,4096]{1,0:T(2,128)}, u32[]{:S(2)}) copy-start(f32[2,4096]{1,0:T(2,128)} %gains.11) | copy-start | bytes 98308
  60.5 4.2 %copy-start.1 = (bf16[4352,256]{1,0:T(8,128)(2,1)S(1)}, bf16[4352,256]{1,0:T(8,128)(2,1)}, u32[]{:S(2)}) copy-start(bf16[4352,256]{1,0:T(8,128)(2,1)} %all-gather.9.cloned.1.call-done) | copy-start | bytes 6684676
  61.0 7.4 %copy-start.10 = (f32[2,128]{1,0:T(2,128)S(1)}, f32[2,128]{1,0:T(2,128)}, u32[]{:S(2)}) copy-start(f32[2,128]{1,0:T(2,128)} %bias.3) | copy-start | bytes 3076
  61.0 7.4 %collective-permute-start = (bf16[32,128]{1,0:T(8,128)(2,1)S(1)}, bf16[32,128]{1,0:T(8,128)(2,1)S(1)}, u32[]{:S(2)}, u32[]{:S(2)}) collective-permute-start(bf16[32,128]{1,0:T(8,128)(2,1)S(1)} %shard_map.94), channel_id=1, source_target_pairs={{0,16},{16,32},{32,48},{48,64},{64,80},{80,96},{96,112},{112,128},... | collective-permute-start | bytes 24584 | tf_op jit(solution)/shard_map/ppermute | solution.py:307
  69.9 19.4 %all-to-all-start.2 = ((bf16[8,272,128]{2,1,0:T(8,128)(2,1)}), bf16[8,272,128]{2,1,0:T(8,128)(2,1)S(1)}, u32[]{:S(2)}, u32[]{:S(2)}) async-start(bf16[8,272,128]{2,1,0:T(8,128)(2,1)} %shard_map.96), calls=%async_computation.2 | async-start | bytes 1114112 | tf_op jit(solution)/shard_map/all_to_all | solution.py:27
  76.8 70.0 %all-gather.13.cloned.1.call-start = ((), (), s32[]{:S(2)}) async-start(), calls=%async_computation.7 | async-start | bytes 2621440 | tf_op jit(solution)/shard_map/all_gather | solution.py:303
  76.8 30.8 %collective-permute-start.7 = (bf16[3,192,256]{2,1,0:T(8,128)(2,1)S(1)}, bf16[3,192,256]{2,1,0:T(8,128)(2,1)S(1)}, u32[]{:S(2)}, u32[]{:S(2)}) collective-permute-start(bf16[3,192,256]{2,1,0:T(8,128)(2,1)S(1)} %get-tuple-element.20.three), channel_id=1, source_target_pairs={{0,448},{64,0},{128,64},{192,128},{256,192},{320,256},{384,320},{4... | collective-permute-start | bytes 884744 | tf_op jit(solution)/shard_map/ppermute | solution.py:32
  89.4 21.4 %collective-permute-start.1 = (bf16[8,272,128]{2,1,0:T(8,128)(2,1)S(1)}, bf16[8,272,128]{2,1,0:T(8,128)(2,1)S(1)}, u32[]{:S(2)}, u32[]{:S(2)}) collective-permute-start(bf16[8,272,128]{2,1,0:T(8,128)(2,1)S(1)} %all-to-all-done.2.own), channel_id=1, source_target_pairs={{0,1},{1,0},{2,3},{3,2},{4,5},{5,4},{6,7},{7,6},{8,9},{9,8},{10,11... | collective-permute-start | bytes 1671176 | tf_op jit(solution)/shard_map/ppermute | solution.py:32
  99.2 8.3 %collective-permute-start.6 = (bf16[2,192,256]{2,1,0:T(8,128)(2,1)S(1)}, bf16[2,192,256]{2,1,0:T(8,128)(2,1)S(1)}, u32[]{:S(2)}, u32[]{:S(2)}) collective-permute-start(bf16[2,192,256]{2,1,0:T(8,128)(2,1)S(1)} %get-tuple-element.21), channel_id=1, source_target_pairs={{0,64},{64,128},{128,192},{192,256},{256,320},{320,384},{384,448},... | collective-permute-start | bytes 589832 | tf_op jit(solution)/shard_map/ppermute | solution.py:32
  108.4 2.3 %copy-start.5 = (bf16[256,256]{1,0:T(8,128)(2,1)S(1)}, bf16[256,256]{1,0:T(8,128)(2,1)}, u32[]{:S(2)}) copy-start(bf16[256,256]{1,0:T(8,128)(2,1)} %stream.1) | copy-start | bytes 393220
  108.5 71.4 %all-gather.15.cloned.1.call-start = ((), (), s32[]{:S(2)}) async-start(), calls=%async_computation.8 | async-start | bytes 1310720 | tf_op jit(solution)/shard_map/all_gather | solution.py:304
  108.5 1.2 copy-start.3
  141.9 7.0 %collective-permute-start.8 = (bf16[8,256,256]{2,1,0:T(8,128)(2,1)S(1)}, bf16[8,256,256]{2,1,0:T(8,128)(2,1)S(1)}, u32[]{:S(2)}, u32[]{:S(2)}) collective-permute-start(bf16[8,256,256]{2,1,0:T(8,128)(2,1)S(1)} %all_to_all.26.own), channel_id=1, source_target_pairs={{0,1},{1,0},{2,3},{3,2},{4,5},{5,4},{6,7},{7,6},{8,9},{9,8},{10,11... | collective-permute-start | bytes 3145736 | tf_op jit(solution)/shard_map/ppermute | solution.py:32
  146.8 1.6 copy-start.2
  149.2 6.5 %collective-permute-start.9 = (bf16[32,128]{1,0:T(8,128)(2,1)S(1)}, bf16[32,128]{1,0:T(8,128)(2,1)S(1)}, u32[]{:S(2)}, u32[]{:S(2)}) collective-permute-start(bf16[32,128]{1,0:T(8,128)(2,1)S(1)} %shard_map.103), channel_id=1, source_target_pairs={{0,16},{16,32},{32,48},{48,64},{64,80},{80,96},{96,112},{112,128},... | collective-permute-start | bytes 24584 | tf_op jit(solution)/shard_map/ppermute | solution.py:307
  175.1 6.3 %collective-permute-start.10 = (bf16[8,272,128]{2,1,0:T(8,128)(2,1)S(1)}, bf16[8,272,128]{2,1,0:T(8,128)(2,1)S(1)}, u32[]{:S(2)}, u32[]{:S(2)}) collective-permute-start(bf16[8,272,128]{2,1,0:T(8,128)(2,1)S(1)} %all_to_all.27.own), channel_id=1, source_target_pairs={{0,1},{1,0},{2,3},{3,2},{4,5},{5,4},{6,7},{7,6},{8,9},{9,8},{10,11... | collective-permute-start | bytes 1671176 | tf_op jit(solution)/shard_map/ppermute | solution.py:32
  179.9 1.2 copy-start.4
Sparse Core Ops, SparseCore 0:
  9.5 46.1 all-gather.8
  59.2 33.1 all-gather.10
  108.6 31.0 all-gather.12
  146.9 22.5 all-gather.14
